TPU v7x, 32 devices: a whole 2x2x4 slice. The times are simulated.
32 devices in a mesh: grp: 2 (over x), st: 4 (over y, core), tp: 4 (over z).
Axes of the slice: x: 2, y: 2, z: 4, core: 2. Of those that a mesh axis runs over, the one named last changes fastest.
Arguments:
- tokens: bfloat16 [8192, 2048], P(('grp', 'st')), parts along dimension 0, may hold values from -6 to 6
- w_query: bfloat16 [2048, 512], P(None, 'tp'), may hold values from -0.125 to 0.125
- w_key: bfloat16 [2048, 512], P(None, 'tp'), may hold values from -0.125 to 0.125
- w_value: bfloat16 [2048, 1024], P(None, 'tp'), may hold values from -0.125 to 0.125
- w_decay: bfloat16 [2048, 512], P(None, 'tp'), may hold values from -0.125 to 0.125
- decay_rate: float32 [512], P('tp'), may hold values from 0.0002 to 0.04
- block_scale: float32 [64], P(('grp', 'st')), parts along dimension 0, may hold values from 0.5 to 2
- w_rquery: bfloat16 [2048, 1024], P(None, 'tp'), may hold values from -0.125 to 0.125
- w_gate: bfloat16 [2048, 1024], P(None, 'tp'), may hold values from -0.125 to 0.125
- w_rkey: bfloat16 [2048, 1024], P(None, 'tp'), may hold values from -0.125 to 0.125
- w_rvalue: bfloat16 [2048, 1024], P(None, 'tp'), may hold values from -3 to 3
- query_gain: float32 [128], replicated, may hold values from 0.1 to 1.9
- key_gain: float32 [128], replicated, may hold values from 0.1 to 1.9
- out_gain: float32 [1024], P('tp'), may hold values from 0.1 to 1.9
- store: bfloat16 [96, 128, 2048], P(('grp', 'st')), parts along dimension 0, may hold values from -6 to 6
- passage_ids: int32 [64, 4], P(('grp', 'st')), parts along dimension 0, may hold values from 0 to 47, as said below
Outputs:
- output: bfloat16 [8192, 1024], P(('grp', 'st'), 'tp'), parts along dimension 0
There are 2 independent parts, one for each index of `grp`. A program takes and returns all parts, laid end to end along the dimension named above; an argument that names none is the same for every part. Nothing has to cross between parts.
Inputs may be any that keep to these rules, and one draw needn't show every extreme that they name: `passage_ids`: passage p is held by index p // 12 of st. The 32 reads of the blocks of one index of st name passages of exactly 4 indices of st, exactly 8 reads of each; among them are always the index before its own and the index half the axis away.
All inputs are finite; a program needn't handle non-finite values.
Results may differ from a plain program's by a relative error of at most 0.0044.
Values may be sent and summed in bfloat16 or wider, within the bound.
A program may use at most 128 MiB of HBM per device.

v0:
```python
import jax
import jax.numpy as jnp
from jax import lax
from jax.sharding import PartitionSpec as P

HEADS = 8
DK = 64
DV = 128
BLK = 128
NPASS = 4


EPS = 1e-06
PRECISE = lax.Precision.HIGHEST


def head_norm(values, gain_row):
    return values * lax.rsqrt(jnp.mean(values * values, axis=-1, keepdims=True) + EPS) * gain_row


def gla_blocks(gla_query, gla_key, gla_value, log_decay):
    head_dim = gla_query.shape[-1]
    block_len = gla_query.shape[1]
    cumulative = jnp.cumsum(log_decay, axis=1)
    query_dec = gla_query * head_dim ** (-0.5) * jnp.exp(cumulative)
    key_dec = gla_key * jnp.exp(-cumulative)
    causal_mask = jnp.arange(block_len)[:, None] >= jnp.arange(block_len)[None, :]
    scores = jnp.einsum("nihd,njhd->nhij", query_dec, key_dec, precision=PRECISE)
    scores = jnp.where(causal_mask, scores, 0.0)
    within = jnp.einsum("nhij,njhv->nihv", scores, gla_value, precision=PRECISE)
    block_total = cumulative[:, -1:]
    update = jnp.einsum(
        "njhd,njhv->nhdv", gla_key * jnp.exp(block_total - cumulative), gla_value, precision=PRECISE
    )
    carry_decay = jnp.exp(block_total[:, 0])

    def advance(carry_state, block_item):
        query_part, state_delta, factor = block_item
        result = jnp.einsum("ihd,hdv->ihv", query_part, carry_state, precision=PRECISE)
        return (factor[..., None] * carry_state + state_delta, result)

    start_state = jnp.zeros((gla_query.shape[2], head_dim, gla_value.shape[-1]), jnp.float32)
    _, carried = lax.scan(advance, start_state, (query_dec, update, carry_decay))
    return within + carried


def on_device(
    tokens,
    w_query,
    w_key,
    w_value,
    w_decay,
    decay_rate,
    block_scale,
    w_rquery,
    w_gate,
    w_rkey,
    w_rvalue,
    query_gain,
    key_gain,
    out_gain,
    store,
    passage_ids,
):
    length = tokens.shape[0]
    num_blocks = length // BLK
    local_heads = w_value.shape[1] // DV
    gla_q = jnp.dot(tokens, w_query, preferred_element_type=jnp.float32)
    gla_k = jnp.dot(tokens, w_key, preferred_element_type=jnp.float32)
    gla_v = jnp.dot(tokens, w_value, preferred_element_type=jnp.float32)
    decay_pre = jnp.dot(tokens, w_decay, preferred_element_type=jnp.float32)
    log_decay = (
        -2.0
        * decay_rate[None, :]
        * jax.nn.sigmoid(decay_pre)
        * jnp.repeat(block_scale, BLK)[:, None]
    )

    def shaped(values, width):
        return values.reshape(num_blocks, BLK, local_heads, width)

    gla_out = gla_blocks(
        shaped(gla_q, DK), shaped(gla_k, DK), shaped(gla_v, DV), shaped(log_decay, DK)
    )
    gla_out = gla_out.reshape(length, local_heads * DV)
    stores_here = store.shape[0]
    passage_rows = store.shape[1]
    width = store.shape[2]
    st_size = lax.axis_size("st")
    request_count = passage_ids.shape[0] * passage_ids.shape[1]
    owner_count = min(st_size, request_count // 2)
    most = request_count // owner_count
    flat_ids = passage_ids.reshape(-1)
    owner_index = flat_ids // stores_here
    local_row = flat_ids % stores_here
    request_index = jnp.arange(request_count, dtype=jnp.int32)
    earlier = (owner_index[:, None] == owner_index[None, :]) & (
        request_index[None, :] < request_index[:, None]
    )
    rank_index = jnp.sum(earlier.astype(jnp.int32), axis=1)
    slot_index = owner_index * most + rank_index
    placed = slot_index[:, None] == jnp.arange(st_size * most, dtype=jnp.int32)[None, :]
    wanted = jnp.sum(jnp.where(placed, local_row[:, None] + 1, 0), axis=0) - 1
    incoming = lax.all_to_all(
        wanted.reshape(st_size, most), "st", split_axis=0, concat_axis=0, tiled=True
    )
    held_rows = jnp.take(store, jnp.maximum(incoming.reshape(-1), 0), axis=0)
    flat_rows = held_rows.reshape(st_size * most * passage_rows, width)
    made_keys = jnp.dot(flat_rows, w_rkey, preferred_element_type=jnp.float32).astype(jnp.bfloat16)
    made_values = jnp.dot(flat_rows, w_rvalue, preferred_element_type=jnp.float32).astype(
        jnp.bfloat16
    )
    made_keys = made_keys.reshape(st_size * most, passage_rows, local_heads * DV)
    made_values = made_values.reshape(st_size * most, passage_rows, local_heads * DV)
    back_keys, back_values = (
        lax.all_to_all(made_keys, "st", split_axis=0, concat_axis=0, tiled=True),
        lax.all_to_all(made_values, "st", split_axis=0, concat_axis=0, tiled=True),
    )
    passage_keys = jnp.take(back_keys, slot_index, axis=0).reshape(
        request_count * passage_rows, local_heads * DV
    )
    passage_values = jnp.take(back_values, slot_index, axis=0).reshape(
        request_count * passage_rows, local_heads * DV
    )
    key_rows = NPASS * passage_rows
    key_normed = head_norm(
        passage_keys.astype(jnp.float32).reshape(num_blocks, key_rows, local_heads, DV), key_gain
    ).astype(jnp.bfloat16)
    value_rows = passage_values.reshape(num_blocks, key_rows, local_heads, DV)
    read_query = jnp.dot(tokens, w_rquery, preferred_element_type=jnp.float32).reshape(
        num_blocks, BLK, local_heads, DV
    )
    read_query = head_norm(read_query, query_gain).astype(jnp.bfloat16)
    scores = jnp.einsum(
        "nqhd,nkhd->nhqk", read_query, key_normed, preferred_element_type=jnp.float32
    ) * DV ** (-0.5)
    expd = jnp.exp(scores)
    read_weight = (expd / jnp.sum(expd, axis=-1, keepdims=True)).astype(jnp.bfloat16)
    retrieved = jnp.einsum(
        "nhqk,nkhd->nqhd", read_weight, value_rows, preferred_element_type=jnp.float32
    )
    retrieved = retrieved.reshape(length, local_heads * DV)
    gate_value = jax.nn.sigmoid(jnp.dot(tokens, w_gate, preferred_element_type=jnp.float32))
    combined = gla_out + gate_value * retrieved
    square_sum = lax.psum(jnp.sum(combined * combined, axis=1), "tp")
    scale_rows = lax.rsqrt(square_sum / (HEADS * DV) + EPS)
    return (combined * scale_rows[:, None] * out_gain[None, :]).astype(jnp.bfloat16)


def solution(mesh):
    return jax.shard_map(
        on_device,
        mesh=mesh,
        in_specs=(
            P(("grp", "st"), None),
            P(None, "tp"),
            P(None, "tp"),
            P(None, "tp"),
            P(None, "tp"),
            P("tp"),
            P(("grp", "st")),
            P(None, "tp"),
            P(None, "tp"),
            P(None, "tp"),
            P(None, "tp"),
            P(),
            P(),
            P("tp"),
            P(("grp", "st"), None, None),
            P(("grp", "st"), None),
        ),
        out_specs=P(("grp", "st"), "tp"),
        check_vma=False,
    )
```

profile of v0, /device:TPU:0, one launch (start us, length us, event | category | flops | bytes accessed | tf_op | source)
XLA Modules:
  0.0 182.8 jit_solution(12584639683676915347)
XLA Ops:
  0.0 0.8 broadcast_divide_fusion
  0.8 0.7 sign_compare_fusion
  2.3 0.7 sub.27
  3.0 4.3 %all-to-all-start = ((s32[4,1,8]{2,1,0:T(1,128)}), s32[4,1,8]{2,1,0:T(1,128)S(1)}, u32[]{:S(2)}, u32[]{:S(2)}) async-start(s32[4,1,8]{2,1,0:T(1,128)} %bitcast.3), calls=%async_computation | async-start | bytes 4096 | tf_op jit(solution)/shard_map/all_to_all | solution.py:104
  7.2 0.7 broadcast_bitcast_fusion.1
  8.0 0.7 broadcast_multiply_fusion
  8.6 3.6 %fusion.25 = f32[1024,128]{1,0:T(8,128)S(1)} fusion(bf16[1024,2048]{1,0:T(8,128)(2,1)} %param.20, bf16[2048,128]{1,0:T(8,128)(2,1)} %param.24, f32[1024]{0:T(1024)S(1)} %broadcast_bitcast_fusion.1, f32[128]{0:T(128)S(1)} %broadcast_multiply_fusion), kind=kOutput, calls=%fused_computation.45 | convolution fusion | flops 537526272 | bytes 5247488 | tf_op jit(solution)/shard_map/dot_general | solution.py:71
  12.2 0.6 reshape.212
  12.8 0.7 fusion.26
  13.5 3.8 %convolution_bitcast_fusion.2 = f32[16,8,8,128]{3,1,2,0:T(8,128)S(1)} fusion(bf16[1024,2048]{1,0:T(8,128)(2,1)} %param.20, bf16[2048,128]{1,0:T(8,128)(2,1)} %param.22), kind=kOutput, calls=%fused_computation.39 | convolution fusion | flops 536870912 | bytes 5242880 | tf_op jit(solution)/shard_map/dot_general | solution.py:69
  17.4 1.4 copy.167
  18.8 3.5 %convolution_multiply_fusion = f32[1024,128]{1,0:T(8,128)S(1)} fusion(bf16[1024,2048]{1,0:T(8,128)(2,1)} %param.20, bf16[2048,128]{1,0:T(8,128)(2,1)} %param.21), kind=kOutput, calls=%fused_computation.38 | convolution fusion | flops 537001984 | bytes 5242880 | tf_op jit(solution)/shard_map/dot_general | solution.py:68
  22.3 1.6 reshape.211
  23.9 4.8 %fusion.38 = f32[1024,256]{1,0:T(8,128)} fusion(bf16[1024,2048]{1,0:T(8,128)(2,1)} %param.20, bf16[2048,256]{1,0:T(8,128)(2,1)} %param.23), kind=kOutput, calls=%fused_computation.90 | convolution fusion | flops 1073741824 | bytes 6291456 | tf_op jit(solution)/shard_map/dot_general | solution.py:70
  28.7 1.7 reshape.171
  30.5 3.7 %exponential_multiply_fusion.1 = (f32[8,128,2,64]{3,0,1,2:T(8,128)}, f32[8,128,2,64]{3,0,1,2:T(8,128)}, f32[8,128,2,64]{3,0,1,2:T(8,128)}) fusion(f32[8,128,2,64]{3,0,1,2:T(8,128)} %copy.167, f32[8,128,2,64]{3,0,1,2:T(8,128)S(1)} %fusion.26, f32[8,2,64]{2,0,1:T(8,128)S(1)} %slice_bitcast_fusion, f32[8,128,2,64]{3,2,1,0:T(2,128)} %reshape.211), kind=kLoop, calls=%fused_computation.57 | loop fusion | flops 655360 | bytes 3149824 | tf_op jit(solution)/shard_map/mul | solution.py:26
  34.2 1.5 copy.168
  35.7 3.2 %fusion.28 = f32[8,2,64,128]{3,2,1,0:T(8,128)S(1)} fusion(f32[8,128,2,64]{3,0,1,2:T(8,128)} %get-tuple-element.117, f32[8,128,2,128]{3,2,1,0:T(2,128)S(1)} %reshape.171), kind=kOutput, calls=%fused_computation.49 | convolution fusion | flops 201326592 | bytes 2097152 | tf_op jit(solution)/shard_map/njhd,njhv->nhdv/dot_general | solution.py:32
  38.9 10.3 %while.13 = (s32[]{:T(128)}, f32[2,64,128]{2,1,0:T(8,128)S(1)}, f32[8,128,2,128]{1,3,2,0:T(8,128)}, f32[8,2,64]{2,0,1:T(8,128)S(1)}, f32[8,2,64,128]{3,2,1,0:T(8...) while((s32[]{:T(128)}, f32[2,64,128]{2,1,0:T(8,128)S(1)}, ...), condition=%wide.region_2.3_spmd.clone, body=%wide.region_1.2_spmd.clone.sunk | while | flops 25231364 | bytes 985196 | solution.py:43
  38.9 0.4 convolution_bitcast_fusion.4
  39.6 0.7 constant_dynamic-update-slice_fusion.2
  40.2 0.4 convolution_bitcast_fusion.4
  40.9 0.7 constant_dynamic-update-slice_fusion.2
  41.5 0.4 convolution_bitcast_fusion.4
  42.1 0.7 constant_dynamic-update-slice_fusion.2
  42.8 0.4 convolution_bitcast_fusion.4
  43.4 0.6 constant_dynamic-update-slice_fusion.2
  44.1 0.4 convolution_bitcast_fusion.4
  44.7 0.7 constant_dynamic-update-slice_fusion.2
  45.4 0.4 convolution_bitcast_fusion.4
  46.0 0.7 constant_dynamic-update-slice_fusion.2
  46.7 0.4 convolution_bitcast_fusion.4
  47.3 0.7 constant_dynamic-update-slice_fusion.2
  48.6 0.7 constant_dynamic-update-slice_fusion.2
  49.6 10.1 %gather_fusion = bf16[32,128,2048]{2,1,0:T(8,128)(2,1)} fusion(bf16[12,128,2048]{2,1,0:T(8,128)(2,1)} %param.34, s32[1024]{0:T(1024)S(1)} %pad_clamp_fusion.1), kind=kCustom, calls=%fused_computation.2 | custom fusion | bytes 33554560 | tf_op jit(solution)/shard_map/jit(_take)/gather | solution.py:107
  59.7 9.1 %bitcast_select_fusion = bf16[4096,2048]{1,0:T(8,128)(2,1)S(1)} fusion(bf16[32,128,2048]{2,1,0:T(8,128)(2,1)} %gather_fusion, pred[4096]{0:T(1024)(128)(4,1)S(1)} %broadcast_bitcast_fusion), kind=kLoop, calls=%fused_computation.14 | loop fusion | flops 8388608 | bytes 33558528 | tf_op jit(solution)/shard_map/jit(_take)/select_n | solution.py:107
  68.8 6.3 %convolution_convert_fusion = bf16[4096,256]{1,0:T(8,128)(2,1)} fusion(bf16[4096,2048]{1,0:T(8,128)(2,1)S(1)} %bitcast_select_fusion, bf16[2048,256]{1,0:T(8,128)(2,1)S(1)} %copy-done), kind=kOutput, calls=%fused_computation.15 | convolution fusion | flops 4296015872 | bytes 19922944 | tf_op jit(solution)/shard_map/dot_general | solution.py:109
  75.2 4.6 %all-to-all-start.2 = ((bf16[32,128,256]{2,1,0:T(8,128)(2,1)}), bf16[32,128,256]{2,1,0:T(8,128)(2,1)}, u32[]{:S(2)}, u32[]{:S(2)}) async-start(bf16[32,128,256]{2,1,0:T(8,128)(2,1)} %bitcast.77), calls=%async_computation.2 | async-start | bytes 4194304 | tf_op jit(solution)/shard_map/all_to_all | solution.py:116
  79.7 3.4 %fusion.39 = f32[1024,256]{1,0:T(8,128)S(1)} fusion(bf16[1024,2048]{1,0:T(8,128)(2,1)} %param.20, bf16[2048,256]{1,0:T(8,128)(2,1)S(1)} %copy-done.14), kind=kOutput, calls=%fused_computation.91 | convolution fusion | flops 1073741824 | bytes 6291456 | tf_op jit(solution)/shard_map/dot_general | solution.py:130
  83.2 0.5 reshape.176
  83.7 1.2 multiply_reduce_fusion.2
  85.1 11.8 %convolution_convert_fusion.1 = bf16[4096,256]{1,0:T(8,128)(2,1)} fusion(bf16[4096,2048]{1,0:T(8,128)(2,1)} %copy-done.2, bf16[2048,256]{1,0:T(8,128)(2,1)} %param.30), kind=kOutput, calls=%fused_computation.16 | convolution fusion | flops 4296015872 | bytes 19922944 | tf_op jit(solution)/shard_map/dot_general | solution.py:110
  96.9 8.5 %all-to-all-done.2 = bf16[32,128,256]{2,1,0:T(8,128)(2,1)} async-done(((bf16[32,128,256]{2,1,0:T(8,128)(2,1)}), bf16[32,128,256]{2,1,0:T(8,128)(2,1)}, u32[]{:S(2)}, u32[]{:S(2)}) %all-to-all-start.2) | async-done | bytes 2097184 | tf_op jit(solution)/shard_map/all_to_all | solution.py:116
  105.5 4.7 %all-to-all-start.1 = ((bf16[32,128,256]{2,1,0:T(8,128)(2,1)}), bf16[32,128,256]{2,1,0:T(8,128)(2,1)}, u32[]{:S(2)}, u32[]{:S(2)}) async-start(bf16[32,128,256]{2,1,0:T(8,128)(2,1)} %bitcast.76), calls=%async_computation.1 | async-start | bytes 4194304 | tf_op jit(solution)/shard_map/all_to_all | solution.py:117
  110.1 1.0 copy.184
  111.2 3.4 %convolution_select_fusion = f32[8,2,128,128]{3,2,1,0:T(8,128)S(1)} fusion(f32[8,128,2,64]{1,3,2,0:T(8,128)} %copy-done.6, f32[8,128,2,64]{3,0,1,2:T(8,128)S(1)} %copy-done.5, pred[128,128]{1,0:T(8,128)(4,1)S(1)} %iota_compare_fusion), kind=kOutput, calls=%fused_computation.33 | convolution fusion | flops 201588736 | bytes 2113536 | tf_op jit(solution)/shard_map/nihd,njhd->nhij/dot_general | solution.py:28
  114.6 3.1 %fusion.16 = f32[8,128,2,128]{1,3,2,0:T(8,128)S(1)} fusion(f32[8,128,2,128]{1,3,2,0:T(8,128)} %get-tuple-element.38, f32[8,2,128,128]{3,2,1,0:T(8,128)S(1)} %convolution_select_fusion, f32[8,128,2,128]{3,2,1,0:T(2,128)S(1)} %reshape.171), kind=kOutput, calls=%fused_computation.32 | convolution fusion | flops 402915328 | bytes 4194304 | tf_op jit(solution)/shard_map/nhij,njhv->nihv/dot_general | solution.py:30
  117.7 1.6 copy.177
  119.3 2.2 %multiply_convert_fusion.2 = bf16[8,128,2,128]{3,2,1,0:T(2,128)(2,1)} fusion(f32[8,128,2,128]{3,2,1,0:T(2,128)S(1)} %reshape.176, f32[128]{0:T(128)S(1)} %copy-done.12, f32[8,128,2]{2,1,0:T(8,128)S(1)} %copy-done.8), kind=kLoop, calls=%fused_computation.54 | loop fusion | flops 786432 | bytes 1581568 | tf_op jit(solution)/shard_map/convert_element_type | solution.py:133
  121.6 2.3 %gather_fusion.2 = bf16[32,128,256]{2,1,0:T(8,128)(2,1)S(1)} fusion(bf16[32,128,256]{2,1,0:T(8,128)(2,1)} %all-to-all-done.2, s32[1024]{0:T(1024)S(1)} %pad_clamp_fusion), kind=kCustom, calls=%fused_computation.1.clone | custom fusion | bytes 4194432 | tf_op jit(solution)/shard_map/jit(_take)/gather | solution.py:119
  123.9 11.8 %all-to-all-done.1 = bf16[32,128,256]{2,1,0:T(8,128)(2,1)} async-done(((bf16[32,128,256]{2,1,0:T(8,128)(2,1)}), bf16[32,128,256]{2,1,0:T(8,128)(2,1)}, u32[]{:S(2)}, u32[]{:S(2)}) %all-to-all-start.1) | async-done | bytes 2097184 | tf_op jit(solution)/shard_map/all_to_all | solution.py:117
  135.6 3.7 %gather_fusion.1 = bf16[32,128,256]{2,1,0:T(8,128)(2,1)} fusion(bf16[32,128,256]{2,1,0:T(8,128)(2,1)} %all-to-all-done.1, s32[1024]{0:T(1024)S(1)} %pad_clamp_fusion), kind=kCustom, calls=%fused_computation.clone | custom fusion | bytes 4194432 | tf_op jit(solution)/shard_map/jit(_take)/gather | solution.py:122
  139.3 4.6 %broadcast_select_fusion = (bf16[32,128,256]{2,1,0:T(8,128)(2,1)}, f32[32,128,256]{2,1,0:T(8,128)}) fusion(bf16[32,128,256]{2,1,0:T(8,128)(2,1)} %gather_fusion.1, pred[32]{0:T(512)(128)(4,1)S(1)} %get-tuple-element.114, bf16[32,128,256]{2,1,0:T(8,128)(2,1)S(1)} %gather_fusion.2), kind=kLoop, calls=%fused_computation.27 | loop fusion | flops 3145728 | bytes 10485792 | tf_op jit(solution)/shard_map/jit(_take)/select_n | solution.py:122
  143.9 5.8 %reshape.214 = f32[8,512,2,128]{3,2,1,0:T(2,128)} reshape(f32[32,128,256]{2,1,0:T(8,128)} %get-tuple-element.122) | data formatting | bytes 8388608 | tf_op jit(solution)/shard_map/convert_element_type | solution.py:127
  149.7 5.3 %copy.198 = f32[8,512,2,128]{1,0,3,2:T(8,128)} copy(f32[8,512,2,128]{3,2,1,0:T(2,128)} %reshape.214) | data formatting | bytes 8388608 | tf_op jit(solution)/shard_map/convert_element_type | solution.py:127
  155.0 2.7 %multiply_reduce_fusion = f32[8,512,2]{1,0,2:T(8,128)S(1)} fusion(f32[8,512,2,128]{1,0,3,2:T(8,128)} %copy.198), kind=kLoop, calls=%fused_computation.20 | loop fusion | flops 2088960 | bytes 4227072 | tf_op jit(solution)/shard_map/reduce_sum | solution.py:18
  157.9 2.1 %reshape.213 = bf16[8,512,2,128]{3,2,1,0:T(2,128)(2,1)} reshape(bf16[32,128,256]{2,1,0:T(8,128)(2,1)S(1)} %copy-done.3) | data formatting | bytes 4194304 | tf_op jit(solution)/shard_map/reshape;reshape | solution.py:129
  159.9 2.7 %multiply_convert_fusion = bf16[8,512,2,128]{1,0,3,2:T(8,128)(2,1)S(1)} fusion(f32[8,512,2,128]{1,0,3,2:T(8,128)} %copy.198, f32[128]{0:T(128)S(1)} %copy-done.13, f32[8,512,2]{1,0,2:T(8,128)S(1)} %add_rsqrt_fusion), kind=kLoop, calls=%fused_computation.19 | loop fusion | flops 3145728 | bytes 6324736 | tf_op jit(solution)/shard_map/convert_element_type | solution.py:128
  162.6 2.1 %fusion.7 = (f32[8,2,128]{2,1,0:T(2,128)S(1)}, f32[8,2,128,512]{3,2,1,0:T(8,128)S(1)}) fusion(bf16[8,512,2,128]{1,0,3,2:T(8,128)(2,1)S(1)} %multiply_convert_fusion, bf16[8,128,2,128]{3,2,1,0:T(2,128)(2,1)S(1)} %copy-done.7), kind=kOutput, calls=%fused_computation.21 | convolution fusion | flops 270530560 | bytes 6823936 | tf_op jit(solution)/shard_map/nqhd,nkhd->nhqk/dot_general | solution.py:134
  164.7 1.7 fusion.12
  166.5 0.6 copy.189
  167.5 1.7 multiply_reduce_fusion.1
  169.2 12.4 %psum.7 = f32[1024]{0:T(1024)S(1)} all-reduce(f32[1024]{0:T(1024)S(1)} %get-tuple-element.127), channel_id=1, replica_groups=mesh['grp'=2,'st'=4,'tp'=4] {'tp'}, use_global_device_ids=true, to_apply=%region_9.11 | all-reduce | flops 1024 | bytes 8192 | tf_op jit(solution)/shard_map/psum | solution.py:145
  181.8 1.0 copy.190
  (88 shorter events, 4.2 us)
Async XLA Ops:
  0.0 68.8 %copy-start = (bf16[2048,256]{1,0:T(8,128)(2,1)S(1)}, bf16[2048,256]{1,0:T(8,128)(2,1)}, u32[]{:S(2)}) copy-start(bf16[2048,256]{1,0:T(8,128)(2,1)} %param.29) | copy-start | bytes 3145732
  3.0 46.3 %all-to-all-start = ((s32[4,1,8]{2,1,0:T(1,128)}), s32[4,1,8]{2,1,0:T(1,128)S(1)}, u32[]{:S(2)}, u32[]{:S(2)}) async-start(s32[4,1,8]{2,1,0:T(1,128)} %bitcast.3), calls=%async_computation | async-start | bytes 4096 | tf_op jit(solution)/shard_map/all_to_all | solution.py:104
  49.3 10.4 %copy-start.6 = (f32[8,128,2,64]{1,3,2,0:T(8,128)}, f32[8,128,2,64]{1,3,2,0:T(8,128)S(1)}, u32[]{:S(2)}) copy-start(f32[8,128,2,64]{1,3,2,0:T(8,128)S(1)} %get-tuple-element.190) | copy-start | bytes 1572868
  68.8 6.3 %copy-start.2 = (bf16[4096,2048]{1,0:T(8,128)(2,1)}, bf16[4096,2048]{1,0:T(8,128)(2,1)S(1)}, u32[]{:S(2)}) copy-start(bf16[4096,2048]{1,0:T(8,128)(2,1)S(1)} %bitcast_select_fusion) | copy-start | bytes 50331652
  75.2 4.6 %copy-start.14 = (bf16[2048,256]{1,0:T(8,128)(2,1)S(1)}, bf16[2048,256]{1,0:T(8,128)(2,1)}, u32[]{:S(2)}) copy-start(bf16[2048,256]{1,0:T(8,128)(2,1)} %param.27) | copy-start | bytes 3145732
  75.2 30.3 %all-to-all-start.2 = ((bf16[32,128,256]{2,1,0:T(8,128)(2,1)}), bf16[32,128,256]{2,1,0:T(8,128)(2,1)}, u32[]{:S(2)}, u32[]{:S(2)}) async-start(bf16[32,128,256]{2,1,0:T(8,128)(2,1)} %bitcast.77), calls=%async_computation.2 | async-start | bytes 4194304 | tf_op jit(solution)/shard_map/all_to_all | solution.py:116
  96.9 14.3 %copy-start.5 = (f32[8,128,2,64]{3,0,1,2:T(8,128)S(1)}, f32[8,128,2,64]{3,0,1,2:T(8,128)}, u32[]{:S(2)}) copy-start(f32[8,128,2,64]{3,0,1,2:T(8,128)} %get-tuple-element.116) | copy-start | bytes 1572868
  105.5 30.2 %all-to-all-start.1 = ((bf16[32,128,256]{2,1,0:T(8,128)(2,1)}), bf16[32,128,256]{2,1,0:T(8,128)(2,1)}, u32[]{:S(2)}, u32[]{:S(2)}) async-start(bf16[32,128,256]{2,1,0:T(8,128)(2,1)} %bitcast.76), calls=%async_computation.1 | async-start | bytes 4194304 | tf_op jit(solution)/shard_map/all_to_all | solution.py:117
  111.2 8.1 %copy-start.8 = (f32[8,128,2]{2,1,0:T(8,128)S(1)}, f32[8,128,2]{2,1,0:T(8,128)}, u32[]{:S(2)}) copy-start(f32[8,128,2]{2,1,0:T(8,128)} %copy.184) | copy-start | bytes 24580
  111.2 8.1 %copy-start.12 = (f32[128]{0:T(128)S(1)}, f32[128]{0:T(128)}, u32[]{:S(2)}) copy-start(f32[128]{0:T(128)} %param.31) | copy-start | bytes 1540
  155.0 2.9 %copy-start.3 = (bf16[32,128,256]{2,1,0:T(8,128)(2,1)S(1)}, bf16[32,128,256]{2,1,0:T(8,128)(2,1)}, u32[]{:S(2)}) copy-start(bf16[32,128,256]{2,1,0:T(8,128)(2,1)} %get-tuple-element.121) | copy-start | bytes 6291460
  155.0 4.9 %copy-start.13 = (f32[128]{0:T(128)S(1)}, f32[128]{0:T(128)}, u32[]{:S(2)}) copy-start(f32[128]{0:T(128)} %param.32) | copy-start | bytes 1540
  159.9 2.7 %copy-start.7 = (bf16[8,128,2,128]{3,2,1,0:T(2,128)(2,1)S(1)}, bf16[8,128,2,128]{3,2,1,0:T(2,128)(2,1)}, u32[]{:S(2)}) copy-start(bf16[8,128,2,128]{3,2,1,0:T(2,128)(2,1)} %multiply_convert_fusion.2) | copy-start | bytes 1572868
  162.6 2.1 %copy-start.9 = (bf16[8,512,2,128]{3,2,1,0:T(2,128)(2,1)S(1)}, bf16[8,512,2,128]{3,2,1,0:T(2,128)(2,1)}, u32[]{:S(2)}) copy-start(bf16[8,512,2,128]{3,2,1,0:T(2,128)(2,1)} %reshape.213) | copy-start | bytes 6291460
  164.7 2.4 %copy-start.4 = (bf16[1024,2048]{1,0:T(8,128)(2,1)S(1)}, bf16[1024,2048]{1,0:T(8,128)(2,1)}, u32[]{:S(2)}) copy-start(bf16[1024,2048]{1,0:T(8,128)(2,1)} %param.20) | copy-start | bytes 12582916
  164.7 2.5 %copy-start.10 = (f32[8,128,2,128]{1,0,3,2:T(8,128)S(1)}, f32[8,128,2,128]{1,0,3,2:T(8,128)}, u32[]{:S(2)}) copy-start(f32[8,128,2,128]{1,0,3,2:T(8,128)} %copy.177) | copy-start | bytes 3145732
  164.7 2.8 %copy-start.15 = (bf16[2048,256]{1,0:T(8,128)(2,1)S(1)}, bf16[2048,256]{1,0:T(8,128)(2,1)}, u32[]{:S(2)}) copy-start(bf16[2048,256]{1,0:T(8,128)(2,1)} %param.28) | copy-start | bytes 3145732
  167.5 14.1 %copy-start.11 = (f32[256]{0:T(256)S(1)}, f32[256]{0:T(256)}, u32[]{:S(2)}) copy-start(f32[256]{0:T(256)} %param.33) | copy-start | bytes 3076
  167.5 15.3 %copy-start.1 = (bf16[2048,256]{1,0:T(8,128)(2,1)S(1)}, bf16[2048,256]{1,0:T(8,128)(2,1)}, u32[]{:S(2)}) copy-start(bf16[2048,256]{1,0:T(8,128)(2,1)} %param.29) | copy-start | bytes 3145732
where the time goes:
time: 184 us; the launch traced here: 183 us
  matrix products  55.6 us (30%)
  local copies, waits for them, and re-layouts  50 us (27%)
  other arithmetic  30.3 us (16%)
  waiting for transfers between devices  20.3 us (11%)
  starting transfers between devices  13.5 us (7%)
  blocking collectives  12.4 us (7%)
    psum x1, blocking collectives, on_device(): square_sum = lax.psum(jnp.sum(combined * combined, axis=1), 'tp')  12.4 us
    dot_general x1, matrix products, on_device(): jnp.dot(flat_rows, w_rvalue, preferred_element_type=jnp.float32)  11.8 us
    all_to_all x1, waiting for transfers between devices, on_device(): lax.all_to_all(made_values, 'st', split_axis=0, concat_axis=0, tiled=True)  11.8 us
    convert_element_type x2, local copies, waits for them, and re-layouts, on_device(): passage_keys.astype(jnp.float32)  11.1 us
    gather x1, local copies, waits for them, and re-layouts, on_device(): held_rows = jnp.take(store, jnp.maximum(incoming.reshape(-1), 0), axis=0)  10.1 us
    select_n x1, other arithmetic, on_device(): held_rows = jnp.take(store, jnp.maximum(incoming.reshape(-1), 0), axis=0)  9.14 us
    all_to_all x1, waiting for transfers between devices, on_device(): lax.all_to_all(made_keys, 'st', split_axis=0, concat_axis=0, tiled=True)  8.53 us
    dot_general x1, matrix products, on_device(): jnp.dot(flat_rows, w_rkey, preferred_element_type=jnp.float32)  6.33 us
  transfers between devices with their start and end apart: 3, of which 2 were waited for; matrix products, arithmetic and copies ran while one was open for 40% of the time, Pallas kernels for 0%

commit v1 on v0

v1 whole, which is shorter than its diff:
```python
import functools

import jax
import jax.numpy as jnp
from jax import lax
from jax.experimental import pallas as pl
from jax.experimental.pallas import tpu as pltpu
from jax.sharding import PartitionSpec as P

HEADS = 8
DK = 64
DV = 128
BLK = 128
NPASS = 4
PAIR = 2
EPS = 1e-06
PRECISE = lax.Precision.HIGHEST
F32 = jnp.float32
BF16 = jnp.bfloat16
MESH = pl.DeviceIdType.MESH
NT = (((1,), (1,)), ((), ()))
TN = (((0,), (0,)), ((), ()))


def head_norm(values, gain_row):
    return values * lax.rsqrt(jnp.mean(values * values, axis=-1, keepdims=True) + EPS) * gain_row


def query_kernel(tok_ref, w_ref, gain_ref, out_ref):
    made = jnp.dot(tok_ref[...], w_ref[...], preferred_element_type=F32)
    for h in range(made.shape[1] // DV):
        cols = slice(h * DV, (h + 1) * DV)
        out_ref[:, cols] = head_norm(made[:, cols], gain_ref[...]).astype(BF16)


def passage_kernel(rows_ref, wk_ref, wv_ref, gain_ref, out_ref):
    rows = rows_ref[...]
    width = wk_ref.shape[1]
    keys = jnp.dot(rows, wk_ref[...], preferred_element_type=F32).astype(BF16).astype(F32)
    for h in range(width // DV):
        cols = slice(h * DV, (h + 1) * DV)
        out_ref[:, cols] = head_norm(keys[:, cols], gain_ref[...]).astype(BF16)
    out_ref[:, width:] = jnp.dot(rows, wv_ref[...], preferred_element_type=F32).astype(BF16)


def gla_kernel(
    scale_ref, tok_ref, rate_ref, wq, wk, wd, wv, wg, gla_ref, gate_ref, w_all, state, sems
):
    step = pl.program_id(0)
    dk = wq.shape[1]
    dv = wv.shape[1]

    @pl.when(step == 0)
    def _():
        copies = []
        at = 0
        for i, w in enumerate((wq, wk, wd, wv, wg)):
            copies.append(
                pltpu.make_async_copy(w, w_all.at[:, pl.ds(at, w.shape[1])], sems.at[i])
            )
            at += w.shape[1]
        for copy in copies:
            copy.start()
        state[...] = jnp.zeros_like(state)
        for copy in copies:
            copy.wait()

    made = jnp.dot(tok_ref[...], w_all[...], preferred_element_type=F32)
    gate_ref[...] = jax.nn.sigmoid(made[:, 3 * dk + dv :])
    row_id = lax.broadcasted_iota(jnp.int32, (BLK, BLK), 0)
    col_id = lax.broadcasted_iota(jnp.int32, (BLK, BLK), 1)
    causal = row_id >= col_id
    lower = causal.astype(F32)
    lane_head = lax.broadcasted_iota(jnp.int32, (BLK, dk), 1) // DK
    blocks = tok_ref.shape[0] // BLK
    for i in range(blocks):
        rows = slice(i * BLK, (i + 1) * BLK)
        q, k = made[rows, :dk], made[rows, dk : 2 * dk]
        pre, v = made[rows, 2 * dk : 3 * dk], made[rows, 3 * dk : 3 * dk + dv]
        block_scale = scale_ref[step * blocks + i]
        log_decay = -2.0 * rate_ref[...] * jax.nn.sigmoid(pre) * block_scale
        cum = jnp.dot(lower, log_decay, precision=PRECISE, preferred_element_type=F32)
        total = cum[BLK - 1 : BLK, :]
        q_dec = q * (DK ** (-0.5)) * jnp.exp(cum)
        k_dec = k * jnp.exp(-cum)
        k_up = k * jnp.exp(total - cum)
        held = state[...]
        for h in range(dv // DV):
            cols = slice(h * DV, (h + 1) * DV)
            q_h = jnp.where(lane_head == h, q_dec, 0.0)
            scores = lax.dot_general(q_h, k_dec, NT, precision=PRECISE, preferred_element_type=F32)
            scores = jnp.where(causal, scores, 0.0)
            gla_ref[rows, cols] = jnp.dot(
                scores, v[:, cols], precision=PRECISE, preferred_element_type=F32
            ) + lax.dot_general(q_h, held[cols], NT, precision=PRECISE, preferred_element_type=F32)
        state[...] = held * jnp.exp(total) + lax.dot_general(
            v, k_up, TN, precision=PRECISE, preferred_element_type=F32
        )


def read_kernel(reads, n_st, ids_ref, q_ref, own_ref, other_ref, num_ref, den_ref,
                kv, num_acc, den_acc, list_b, list_r, sems):
    held = own_ref.shape[0]
    width = q_ref.shape[2]
    copies = [
        pltpu.make_async_copy(own_ref, kv.at[pl.ds(0, held)], sems.at[0]),
        pltpu.make_async_copy(other_ref, kv.at[pl.ds(held, held)], sems.at[1]),
    ]
    for copy in copies:
        copy.start()
    me = lax.axis_index("st")
    chip = lax.div(me, PAIR)
    num_acc[...] = jnp.zeros_like(num_acc)
    den_acc[...] = jnp.zeros_like(den_acc)
    count = jnp.int32(0)
    for b in range(ids_ref.shape[0]):
        for j in range(ids_ref.shape[1]):
            name = ids_ref[b, j]
            owner = lax.div(name, held)
            row = name - owner * held
            list_b[count] = jnp.int32(b)
            list_r[count] = jnp.where(owner == me, row, row + held)
            count = count + jnp.where(lax.div(owner, PAIR) == chip, 1, 0)
    for copy in copies:
        copy.wait()
    ones = jnp.ones((8, kv.shape[1]), BF16)
    for r in range(reads):
        b, row = list_b[r], list_r[r]
        for h in range(width // DV):
            cols = slice(h * DV, (h + 1) * DV)
            score = lax.dot_general(
                q_ref[b, :, cols], kv[row, :, cols], NT, preferred_element_type=F32
            )
            expd = jnp.exp(score * (DV ** (-0.5))).astype(BF16)
            num_acc[b, :, cols] += jnp.dot(
                expd, kv[row, :, width + h * DV : width + (h + 1) * DV],
                preferred_element_type=F32,
            )
            den_acc[h, b] += lax.dot_general(ones, expd, NT, preferred_element_type=F32)
    num_ref[...] = num_acc[...].astype(BF16)
    for h in range(width // DV):
        for b in range(q_ref.shape[0]):
            den_ref[h, b : b + 1] = den_acc[h, b, 0:1]


def finish_kernel(parts, n_tp, *refs):
    gla_ref, gate_ref, gain_ref = refs[:3]
    nums, dens = refs[3 : 3 + parts], refs[3 + parts : 3 + 2 * parts]
    out_ref, combined, mine, theirs, send_sems, recv_sems = refs[3 + 2 * parts :]
    me = lax.axis_index("tp")
    barrier = pltpu.get_barrier_semaphore()
    peers = [lax.rem(me + k, n_tp) for k in range(1, n_tp)]
    for peer in peers:
        pl.semaphore_signal(barrier, inc=1, device_id={"tp": peer}, device_id_type=MESH)
    blocks, heads = mine.shape[0], dens[0].shape[0]
    width = out_ref.shape[1]
    inverse = []
    for h in range(heads):
        den = dens[0][h]
        for extra in dens[1:]:
            den = den + extra[h]
        inverse.append(jnp.transpose(1.0 / den, (1, 0)))
    ones = jnp.ones((8, width), F32)
    for b in range(blocks):
        rows = slice(b * BLK, (b + 1) * BLK)
        for h in range(heads):
            cols = slice(h * DV, (h + 1) * DV)
            num = nums[0][b, :, cols].astype(F32)
            for extra in nums[1:]:
                num = num + extra[b, :, cols].astype(F32)
            combined[rows, cols] = (
                gla_ref[rows, cols] + gate_ref[rows, cols] * (num * inverse[h][:, b : b + 1])
            )
        held = combined[rows, :]
        sums = lax.dot_general(ones, held * held, NT, precision=PRECISE, preferred_element_type=F32)
        mine[b : b + 1, :] = sums[0:1]
    pl.semaphore_wait(barrier, n_tp - 1)
    copies = []
    for k, peer in enumerate(peers):
        copies.append(
            pltpu.make_async_remote_copy(
                src_ref=mine,
                dst_ref=theirs.at[k],
                send_sem=send_sems.at[k],
                recv_sem=recv_sems.at[k],
                device_id={"tp": peer},
                device_id_type=MESH,
            )
        )
    for copy in copies:
        copy.start()
    for copy in copies:
        copy.wait()
    total = mine[...]
    for k in range(n_tp - 1):
        total = total + theirs[k]
    scale = jnp.transpose(lax.rsqrt(total / (HEADS * DV) + EPS), (1, 0))
    for b in range(blocks):
        rows = slice(b * BLK, (b + 1) * BLK)
        out_ref[rows, :] = (combined[rows, :] * scale[:, b : b + 1] * gain_ref[...]).astype(BF16)


def cost(flops, moved):
    return pl.CostEstimate(flops=int(flops), bytes_accessed=int(moved), transcendentals=0)


def on_device(n_st, n_tp, tokens, w_query, w_key, w_value, w_decay, decay_rate, block_scale,
              w_rquery, w_gate, w_rkey, w_rvalue, query_gain, key_gain, out_gain, store,
              passage_ids):
    length, depth = tokens.shape
    num_blocks = length // BLK
    width = w_value.shape[1]
    heads = width // DV
    stores_here, passage_rows, _ = store.shape
    tile = 2 * BLK
    whole = lambda *shape: pl.BlockSpec(shape, lambda i, *_: (0,) * len(shape))
    any_spec = pl.BlockSpec(memory_space=pl.ANY)
    vmem = pl.BlockSpec(memory_space=pltpu.VMEM)

    def shift(values, by):
        return lax.ppermute(values, "st", [(s, (s + by) % n_st) for s in range(n_st)])

    read_query = pl.pallas_call(
        query_kernel,
        grid=(length // tile,),
        in_specs=[
            pl.BlockSpec((tile, depth), lambda i: (i, 0)),
            whole(depth, width),
            whole(1, DV),
        ],
        out_specs=pl.BlockSpec((tile, width), lambda i: (i, 0)),
        out_shape=jax.ShapeDtypeStruct((length, width), BF16),
        cost_estimate=cost(2 * length * depth * width, 6e6),
        name="query",
    )(tokens, w_rquery, query_gain.reshape(1, DV)).reshape(num_blocks, BLK, width)

    groups = range(1, n_st // PAIR)
    queries = [read_query] + [shift(read_query, PAIR * k) for k in groups]
    ids = [passage_ids] + [shift(passage_ids, PAIR * k) for k in groups]

    rows = stores_here * passage_rows
    made = pl.pallas_call(
        passage_kernel,
        grid=(rows // tile,),
        in_specs=[
            pl.BlockSpec((tile, depth), lambda i: (i, 0)),
            whole(depth, width),
            whole(depth, width),
            whole(1, DV),
        ],
        out_specs=pl.BlockSpec((tile, 2 * width), lambda i: (i, 0)),
        out_shape=jax.ShapeDtypeStruct((rows, 2 * width), BF16),
        cost_estimate=cost(4 * rows * depth * width, 1e7),
        name="passages",
    )(store.reshape(rows, depth), w_rkey, w_rvalue, key_gain.reshape(1, DV))
    made = made.reshape(stores_here, passage_rows, 2 * width)
    other = lax.ppermute(made, "st", [(s, s ^ 1) for s in range(n_st)])

    request_count = passage_ids.shape[0] * passage_ids.shape[1]
    most = request_count // min(n_st, request_count // 2)
    nums, dens = [], []
    for k, (query, names) in enumerate(zip(queries, ids)):
        num, den = pl.pallas_call(
            functools.partial(read_kernel, PAIR * most, n_st),
            in_specs=[
                pl.BlockSpec(memory_space=pltpu.SMEM), vmem, any_spec, any_spec,
            ],
            out_specs=[vmem, vmem],
            out_shape=[
                jax.ShapeDtypeStruct((num_blocks, BLK, width), BF16),
                jax.ShapeDtypeStruct((heads, num_blocks, BLK), F32),
            ],
            scratch_shapes=[
                pltpu.VMEM((2 * stores_here, passage_rows, 2 * width), BF16),
                pltpu.VMEM((num_blocks, BLK, width), F32),
                pltpu.VMEM((heads, num_blocks, 8, BLK), F32),
                pltpu.SMEM((request_count + 1,), jnp.int32),
                pltpu.SMEM((request_count + 1,), jnp.int32),
                pltpu.SemaphoreType.DMA((2,)),
            ],
            cost_estimate=cost(2e9, 5e6),
            name="reads",
        )(names, query, made, other)
        if k:
            num, den = shift(num, -PAIR * k), shift(den, -PAIR * k)
        nums.append(num)
        dens.append(den)

    spare = -w_query.shape[1] % BLK
    if spare:
        w_query, w_key, w_decay = (
            jnp.pad(w, ((0, 0), (0, spare))) for w in (w_query, w_key, w_decay)
        )
        decay_rate = jnp.pad(decay_rate, (0, spare))
    dk = w_query.shape[1]
    gla_out, gate = pl.pallas_call(
        gla_kernel,
        grid=(length // tile,),
        in_specs=[
            pl.BlockSpec(memory_space=pltpu.SMEM),
            pl.BlockSpec((tile, depth), lambda i: (i, 0)),
            whole(1, dk),
        ]
        + [any_spec] * 5,
        out_specs=[pl.BlockSpec((tile, width), lambda i: (i, 0))] * 2,
        out_shape=[jax.ShapeDtypeStruct((length, width), F32)] * 2,
        scratch_shapes=[
            pltpu.VMEM((depth, 3 * dk + 2 * width), BF16),
            pltpu.VMEM((width, dk), F32),
            pltpu.SemaphoreType.DMA((5,)),
        ],
        cost_estimate=cost(8e9, 1e7),
        name="gla",
    )(block_scale, tokens, decay_rate.reshape(1, dk), w_query, w_key, w_decay, w_value, w_gate)

    return pl.pallas_call(
        functools.partial(finish_kernel, len(nums), n_tp),
        in_specs=[vmem] * (3 + 2 * len(nums)),
        out_specs=vmem,
        out_shape=jax.ShapeDtypeStruct((length, width), BF16),
        scratch_shapes=[
            pltpu.VMEM((length, width), F32),
            pltpu.VMEM((num_blocks, BLK), F32),
            pltpu.VMEM((max(n_tp - 1, 1), num_blocks, BLK), F32),
            pltpu.SemaphoreType.DMA((max(n_tp - 1, 1),)),
            pltpu.SemaphoreType.DMA((max(n_tp - 1, 1),)),
        ],
        compiler_params=pltpu.CompilerParams(collective_id=0, has_side_effects=True),
        cost_estimate=cost(1e9, 6e6),
        name="finish",
    )(gla_out, gate, out_gain.reshape(1, width), *nums, *dens)


def solution(mesh):
    return jax.shard_map(
        functools.partial(on_device, mesh.shape["st"], mesh.shape["tp"]),
        mesh=mesh,
        in_specs=(
            P(("grp", "st"), None),
            P(None, "tp"),
            P(None, "tp"),
            P(None, "tp"),
            P(None, "tp"),
            P("tp"),
            P(("grp", "st")),
            P(None, "tp"),
            P(None, "tp"),
            P(None, "tp"),
            P(None, "tp"),
            P(),
            P(),
            P("tp"),
            P(("grp", "st"), None, None),
            P(("grp", "st"), None),
        ),
        out_specs=P(("grp", "st"), "tp"),
        check_vma=False,
    )
```

time: 184 us -> 81.3 us (0.44)
  Pallas kernels: 0 us -> 58.1 us
  matrix products: 55.6 us -> 0 us
  local copies, waits for them, and re-layouts: 50 us -> 4.68 us
  other arithmetic: 30.3 us -> 0 us
  blocking collectives: 12.4 us -> 0 us
  starting transfers between devices: 13.5 us -> 5.19 us
  waiting for transfers between devices: 20.3 us -> 12.8 us
    pallas_call x0 -> x6, Pallas kernels: none -> 58.1 us  [the longest x2 17.8 us: on_device(): pl.pallas_call(functools.partial(read_kernel, PAIR * most, n_st), in_spec...]
    dot_general x21 -> x0, matrix products: 55.6 us -> none  [the longest x1 11.8 us: on_device(): jnp.dot(flat_rows, w_rvalue, preferred_element_type=jnp.float32)]
    all_to_all x3 -> x0, waiting for transfers between devices: 20.3 us -> none  [the longest x1 11.8 us: on_device(): lax.all_to_all(made_values, 'st', split_axis=0, concat_axis=0, tiled=True)]
    gather x3 -> x0, local copies, waits for them, and re-layouts: 16 us -> none  [the longest x1 10.1 us: on_device(): held_rows = jnp.take(store, jnp.maximum(incoming.reshape(-1), 0), axis=0)]
    select_n x4 -> x0, other arithmetic: 13.8 us -> none  [the longest x1 9.14 us: on_device(): held_rows = jnp.take(store, jnp.maximum(incoming.reshape(-1), 0), axis=0)]
    all_to_all x3 -> x0, starting transfers between devices: 13.5 us -> none  [the longest x1 4.66 us: on_device(): lax.all_to_all(made_values, 'st', split_axis=0, concat_axis=0, tiled=True)]
    ppermute x0 -> x5, waiting for transfers between devices: none -> 12.8 us  [the longest x4 12.8 us: shift(): lax.ppermute(values, 'st', [(s, (s + by) % n_st) for s in range(n_st)])]
    psum x1 -> x0, blocking collectives: 12.4 us -> none  [on_device(): square_sum = lax.psum(jnp.sum(combined * combined, axis=1), 'tp')]
  transfers between devices with their start and end apart: 3 -> 5, of which waited for: 2 -> 1; matrix products, arithmetic and copies ran while one was open for 40% -> 0% of each run, Pallas kernels for 0% -> 38%
where the time goes in v1:
time: 81.3 us; the launch traced here: 80.9 us
  Pallas kernels  58.1 us (71%)
  waiting for transfers between devices  12.8 us (16%)
  starting transfers between devices  5.19 us (6%)
  local copies, waits for them, and re-layouts  4.68 us (6%)
    pallas_call x2, Pallas kernels, on_device(): pl.pallas_call(functools.partial(read_kernel, PAIR * most, n_st), in_spec...  17.8 us
    pallas_call x1, Pallas kernels, on_device(): pl.pallas_call(gla_kernel, grid=(length // tile,), in_specs=[pl.BlockSpec...  16.7 us
    ppermute x4, waiting for transfers between devices, shift(): lax.ppermute(values, 'st', [(s, (s + by) % n_st) for s in range(n_st)])  12.8 us
    pallas_call x1, Pallas kernels, on_device(): pl.pallas_call(functools.partial(finish_kernel, len(nums), n_tp), in_spec...  9.76 us
    pallas_call x1, Pallas kernels, on_device(): pl.pallas_call(passage_kernel, grid=(rows // tile,), in_specs=[pl.BlockSp...  8.62 us
    pallas_call x1, Pallas kernels, on_device(): pl.pallas_call(query_kernel, grid=(length // tile,), in_specs=[pl.BlockSp...  5.21 us
    ppermute x4, starting transfers between devices, shift(): lax.ppermute(values, 'st', [(s, (s + by) % n_st) for s in range(n_st)])  4.69 us
    unnamed x18, local copies, waits for them, and re-layouts  4.68 us
  transfers between devices with their start and end apart: 5, of which 1 were waited for; matrix products, arithmetic and copies ran while one was open for 0% of the time, Pallas kernels for 38%

profile of v1, /device:TPU:0, one launch (start us, length us, event | category | flops | bytes accessed | tf_op | source)
XLA Modules:
  0.0 80.9 jit_solution(3244634961419143508)
XLA Ops:
  0.0 8.6 %passages.1 = bf16[1536,512]{1,0:T(8,128)(2,1)} custom-call(bf16[1536,2048]{1,0:T(8,128)(2,1)} %bitcast.10, bf16[2048,256]{1,0:T(8,128)(2,1)} %wk_ref.1, bf16[2048,256]{1,0:T(8,128)(2,1)} %wv_ref.1, f32[1,128]{1,0:T(1,128)} %bitcast.15), custom_call_target="tpu_custom_call" | custom-call | flops 3221225472 | bytes 10000000 | tf_op jit(solution)/shard_map/passages/pallas_call | solution.py:242
  8.6 0.0 copy-start.1
  8.6 0.5 collective-permute-start
  9.1 5.2 %query.1 = bf16[1024,256]{1,0:T(8,128)(2,1)} custom-call(bf16[1024,2048]{1,0:T(8,128)(2,1)} %tok_ref.3, bf16[2048,256]{1,0:T(8,128)(2,1)} %w_ref.1, f32[1,128]{1,0:T(1,128)} %bitcast.9), custom_call_target="tpu_custom_call" | custom-call | flops 1073741824 | bytes 6000000 | tf_op jit(solution)/shard_map/query/pallas_call | solution.py:223
  14.3 2.5 %collective-permute-start.2 = (bf16[8,128,256]{2,1,0:T(8,128)(2,1)}, bf16[8,128,256]{2,1,0:T(8,128)(2,1)S(1)}, u32[]{:S(2)}, u32[]{:S(2)}) collective-permute-start(bf16[8,128,256]{2,1,0:T(8,128)(2,1)} %bitcast.7), channel_id=1, source_target_pairs={{0,8},{4,12},{8,0},{12,4},{1,9},{5,13},{9,1},{13,5},{2,10},{6,14},... | collective-permute-start | bytes 1572872 | tf_op jit(solution)/shard_map/ppermute | solution.py:221
  16.8 0.0 copy-done.1
  16.8 0.1 copy.17.ids_ref
  16.9 0.0 copy-start
  16.9 0.0 collective-permute-start.1
  16.9 12.8 %collective-permute-done.1.ids_ref = s32[8,4]{1,0:T(8,128)S(1)} collective-permute-done((s32[8,4]{1,0:T(8,128)S(1)}, s32[8,4]{1,0:T(8,128)S(1)}, u32[]{:S(2)}, u32[]{:S(2)}) %collective-permute-start.1) | collective-permute-done | bytes 160 | tf_op jit(solution)/shard_map/ppermute | solution.py:221
  29.7 0.0 copy-start.7
  29.7 0.0 collective-permute-done.2.q_ref
  29.7 0.0 copy-start.4
  29.7 0.0 collective-permute-done.other_ref
  29.7 0.6 copy-done.7
  30.3 0.2 copy-done.4
  30.5 0.0 copy-start.2
  30.5 1.1 %copy-done.2 = bf16[12,128,512]{2,1,0:T(8,128)(2,1)} copy-done((bf16[12,128,512]{2,1,0:T(8,128)(2,1)}, bf16[12,128,512]{2,1,0:T(8,128)(2,1)S(1)}, u32[]{:S(2)}) %copy-start.2) | copy-done | bytes 1572888
  31.7 8.9 %reads.3 = (bf16[8,128,256]{2,1,0:T(8,128)(2,1)}, f32[2,8,128]{2,1,0:T(8,128)}) custom-call(s32[8,4]{1,0:T(8,128)} %copy-done.7, bf16[8,128,256]{2,1,0:T(8,128)(2,1)} %copy-done.4, bf16[12,128,512]{2,1,0:T(8,128)(2,1)} %bitcast.12, bf16[12,128,512]{2,1,0:T(8,128)(2,1)} %copy-done.2), custom_call_target="tpu_custom_call" | custom-call | flops 2000000000 | bytes 5000000 | tf_op jit(solution)/shard_map/reads/pallas_call | solution.py:263
  40.6 1.8 %collective-permute-start.3 = (bf16[8,128,256]{2,1,0:T(8,128)(2,1)}, bf16[8,128,256]{2,1,0:T(8,128)(2,1)S(1)}, u32[]{:S(2)}, u32[]{:S(2)}) collective-permute-start(bf16[8,128,256]{2,1,0:T(8,128)(2,1)} %get-tuple-element.14), channel_id=1, source_target_pairs={{0,8},{4,12},{8,0},{12,4},{1,9},{5,13},{9,1},{13,5},{2,10},{6,14},... | collective-permute-start | bytes 1572872 | tf_op jit(solution)/shard_map/ppermute | solution.py:221
  42.4 0.0 copy-start.5
  42.4 16.7 %gla.1 = (f32[1024,256]{1,0:T(8,128)}, f32[1024,256]{1,0:T(8,128)}) custom-call(f32[8]{0:T(128)} %scale_ref.1, bf16[1024,2048]{1,0:T(8,128)(2,1)} %tok_ref.3, f32[1,128]{1,0:T(1,128)} %bitcast.16, bf16[2048,128]{1,0:T(8,128)(2,1)} %wq.1, bf16[2048,128]{1,0:T(8,128)(2,1)} %wk.1, bf16[2048,128]{1,0:T(8,128)(2,1)} %wd.1, bf16[2048,256]{1,0:T(8,128)(2,1)} %wv.1, ...), custom_call_target="tpu_custom_call" | custom-call | flops 8000000000 | bytes 10000000 | tf_op jit(solution)/shard_map/gla/pallas_call | solution.py:296
  59.1 0.0 copy-done
  59.1 0.0 copy-done.5
  59.1 0.4 collective-permute-start.4
  59.5 8.9 %reads.2 = (bf16[8,128,256]{2,1,0:T(8,128)(2,1)}, f32[2,8,128]{2,1,0:T(8,128)}) custom-call(s32[8,4]{1,0:T(8,128)} %copy-done, bf16[8,128,256]{2,1,0:T(8,128)(2,1)} %bitcast.8, bf16[12,128,512]{2,1,0:T(8,128)(2,1)} %bitcast.13, bf16[12,128,512]{2,1,0:T(8,128)(2,1)} %copy-done.2), custom_call_target="tpu_custom_call" | custom-call | flops 2000000000 | bytes 5000000 | tf_op jit(solution)/shard_map/reads/pallas_call | solution.py:263
  68.4 0.0 collective-permute-done.4.refs_6_
  68.4 0.0 copy-start.6
  68.4 0.0 collective-permute-done.3.refs_4_
  68.4 0.0 copy-start.3
  68.4 0.6 copy-done.6
  69.0 0.2 copy-done.3
  69.2 9.8 %finish.1 = bf16[1024,256]{1,0:T(8,128)(2,1)} custom-call(f32[1024,256]{1,0:T(8,128)} %get-tuple-element.11.refs_0_, f32[1024,256]{1,0:T(8,128)} %get-tuple-element.12.refs_1_, f32[1,256]{1,0:T(1,128)} %bitcast.14, bf16[8,128,256]{2,1,0:T(8,128)(2,1)} %get-tuple-element.13.refs_3_, bf16[8,128,256]{2,1,0:T(8,128)(2,1)} %copy-done.3, ...), custom_call_target="tpu_custom_call" | custom-call | flops 1000000000 | bytes 6000000 | tf_op jit(solution)/shard_map/finish/pallas_call | solution.py:316
  79.0 1.9 %copy.20 = bf16[1024,256]{1,0:T(8,128)(2,1)} copy(bf16[1024,256]{1,0:T(8,128)(2,1)} %finish.1) | data formatting | bytes 1048576
Async XLA Ops:
  8.6 8.2 %copy-start.1 = (s32[8,4]{0,1:T(4,128)S(1)}, s32[8,4]{0,1:T(4,128)}, u32[]{:S(2)}) copy-start(s32[8,4]{0,1:T(4,128)} %param.31) | copy-start | bytes 388
  8.6 21.1 %collective-permute-start = (bf16[12,128,512]{2,1,0:T(8,128)(2,1)}, bf16[12,128,512]{2,1,0:T(8,128)(2,1)S(1)}, u32[]{:S(2)}, u32[]{:S(2)}) collective-permute-start(bf16[12,128,512]{2,1,0:T(8,128)(2,1)} %bitcast.11), channel_id=1, source_target_pairs={{0,4},{4,0},{8,12},{12,8},{1,5},{5,1},{9,13},{13,9},{2,6},{6,2},{1... | collective-permute-start | bytes 4718600 | tf_op jit(solution)/shard_map/ppermute | solution.py:257
  14.3 15.4 %collective-permute-start.2 = (bf16[8,128,256]{2,1,0:T(8,128)(2,1)}, bf16[8,128,256]{2,1,0:T(8,128)(2,1)S(1)}, u32[]{:S(2)}, u32[]{:S(2)}) collective-permute-start(bf16[8,128,256]{2,1,0:T(8,128)(2,1)} %bitcast.7), channel_id=1, source_target_pairs={{0,8},{4,12},{8,0},{12,4},{1,9},{5,13},{9,1},{13,5},{2,10},{6,14},... | collective-permute-start | bytes 1572872 | tf_op jit(solution)/shard_map/ppermute | solution.py:221
  16.9 42.2 %copy-start = (s32[8,4]{1,0:T(8,128)}, s32[8,4]{1,0:T(8,128)S(1)}, u32[]{:S(2)}) copy-start(s32[8,4]{1,0:T(8,128)S(1)} %copy.17.ids_ref) | copy-start | bytes 388
  16.9 12.8 %collective-permute-start.1 = (s32[8,4]{1,0:T(8,128)S(1)}, s32[8,4]{1,0:T(8,128)S(1)}, u32[]{:S(2)}, u32[]{:S(2)}) collective-permute-start(s32[8,4]{1,0:T(8,128)S(1)} %copy.17.ids_ref), channel_id=1, source_target_pairs={{0,8},{4,12},{8,0},{12,4},{1,9},{5,13},{9,1},{13,5},{2,10},{6,14},... | collective-permute-start | bytes 392 | tf_op jit(solution)/shard_map/ppermute | solution.py:221
  29.7 0.6 copy-start.7
  29.7 0.8 copy-start.4
  30.5 1.1 %copy-start.2 = (bf16[12,128,512]{2,1,0:T(8,128)(2,1)}, bf16[12,128,512]{2,1,0:T(8,128)(2,1)S(1)}, u32[]{:S(2)}) copy-start(bf16[12,128,512]{2,1,0:T(8,128)(2,1)S(1)} %collective-permute-done.other_ref) | copy-start | bytes 4718596
  40.6 27.8 %collective-permute-start.3 = (bf16[8,128,256]{2,1,0:T(8,128)(2,1)}, bf16[8,128,256]{2,1,0:T(8,128)(2,1)S(1)}, u32[]{:S(2)}, u32[]{:S(2)}) collective-permute-start(bf16[8,128,256]{2,1,0:T(8,128)(2,1)} %get-tuple-element.14), channel_id=1, source_target_pairs={{0,8},{4,12},{8,0},{12,4},{1,9},{5,13},{9,1},{13,5},{2,10},{6,14},... | collective-permute-start | bytes 1572872 | tf_op jit(solution)/shard_map/ppermute | solution.py:221
  42.4 16.8 %copy-start.5 = (f32[2,8,128]{2,1,0:T(8,128)S(1)}, f32[2,8,128]{2,1,0:T(8,128)}, u32[]{:S(2)}) copy-start(f32[2,8,128]{2,1,0:T(8,128)} %get-tuple-element.16) | copy-start | bytes 24580
  59.1 9.3 %collective-permute-start.4 = (f32[2,8,128]{2,1,0:T(8,128)S(1)}, f32[2,8,128]{2,1,0:T(8,128)S(1)}, u32[]{:S(2)}, u32[]{:S(2)}) collective-permute-start(f32[2,8,128]{2,1,0:T(8,128)S(1)} %copy-done.5), channel_id=1, source_target_pairs={{0,8},{4,12},{8,0},{12,4},{1,9},{5,13},{9,1},{13,5},{2,10},{6,14},... | collective-permute-start | bytes 24584 | tf_op jit(solution)/shard_map/ppermute | solution.py:221
  68.4 0.6 copy-start.6
  68.4 0.8 copy-start.3

commit v2 on v1

--- a/solution.py
+++ b/solution.py
@@ -7,14 +7,13 @@
 from jax.experimental.pallas import tpu as pltpu
 from jax.sharding import PartitionSpec as P
 
+
 HEADS = 8
 DK = 64
 DV = 128
 BLK = 128
-NPASS = 4
 PAIR = 2
 EPS = 1e-06
-PRECISE = lax.Precision.HIGHEST
 F32 = jnp.float32
 BF16 = jnp.bfloat16
 MESH = pl.DeviceIdType.MESH
@@ -24,6 +23,11 @@
 
 def head_norm(values, gain_row):
     return values * lax.rsqrt(jnp.mean(values * values, axis=-1, keepdims=True) + EPS) * gain_row
+
+
+def split(values):
+    high = values.astype(BF16)
+    return high, (values - high.astype(F32)).astype(BF16)
 
 
 def query_kernel(tok_ref, w_ref, gain_ref, out_ref):
@@ -71,6 +75,7 @@
     col_id = lax.broadcasted_iota(jnp.int32, (BLK, BLK), 1)
     causal = row_id >= col_id
     lower = causal.astype(F32)
+    lower = jnp.concatenate([lower, lower], axis=1).astype(BF16)
     lane_head = lax.broadcasted_iota(jnp.int32, (BLK, dk), 1) // DK
     blocks = tok_ref.shape[0] // BLK
     for i in range(blocks):
@@ -79,26 +84,39 @@
         pre, v = made[rows, 2 * dk : 3 * dk], made[rows, 3 * dk : 3 * dk + dv]
         block_scale = scale_ref[step * blocks + i]
         log_decay = -2.0 * rate_ref[...] * jax.nn.sigmoid(pre) * block_scale
-        cum = jnp.dot(lower, log_decay, precision=PRECISE, preferred_element_type=F32)
+        high, low = split(log_decay)
+        cum = jnp.dot(
+            lower, jnp.concatenate([high, low], axis=0), preferred_element_type=F32
+        )
         total = cum[BLK - 1 : BLK, :]
-        q_dec = q * (DK ** (-0.5)) * jnp.exp(cum)
         k_dec = k * jnp.exp(-cum)
-        k_up = k * jnp.exp(total - cum)
+        q_high, q_low = split(q * (DK ** (-0.5)) * jnp.exp(cum))
+        k_high, k_low = split(k_dec)
+        k_twice = jnp.concatenate([k_high, k_high], axis=1)
+        up = jnp.concatenate(split(k * jnp.exp(total - cum)), axis=1)
+        v_high = v.astype(BF16)
+        v_twice = jnp.concatenate([v_high, v_high], axis=0)
         held = state[...]
+        held_high = held.astype(BF16)
+        held_twice = jnp.concatenate([held_high, held_high], axis=1)
         for h in range(dv // DV):
             cols = slice(h * DV, (h + 1) * DV)
-            q_h = jnp.where(lane_head == h, q_dec, 0.0)
-            scores = lax.dot_general(q_h, k_dec, NT, precision=PRECISE, preferred_element_type=F32)
-            scores = jnp.where(causal, scores, 0.0)
+            mine = lane_head == h
+            zero = jnp.zeros((), BF16)
+            own_high = jnp.where(mine, q_high, zero)
+            q_h = jnp.concatenate([own_high, jnp.where(mine, q_low, zero)], axis=1)
+            scores = lax.dot_general(
+                q_h, k_twice, NT, preferred_element_type=F32
+            ) + lax.dot_general(own_high, k_low, NT, preferred_element_type=F32)
+            scores = jnp.concatenate(split(jnp.where(causal, scores, 0.0)), axis=1)
             gla_ref[rows, cols] = jnp.dot(
-                scores, v[:, cols], precision=PRECISE, preferred_element_type=F32
-            ) + lax.dot_general(q_h, held[cols], NT, precision=PRECISE, preferred_element_type=F32)
-        state[...] = held * jnp.exp(total) + lax.dot_general(
-            v, k_up, TN, precision=PRECISE, preferred_element_type=F32
-        )
-
-
-def read_kernel(reads, n_st, ids_ref, q_ref, own_ref, other_ref, num_ref, den_ref,
+                scores, v_twice[:, cols], preferred_element_type=F32
+            ) + lax.dot_general(q_h, held_twice[cols], NT, preferred_element_type=F32)
+        added = lax.dot_general(v_high, up, TN, preferred_element_type=F32)
+        state[...] = held * jnp.exp(total) + added[:, :dk] + added[:, dk:]
+
+
+def read_kernel(reads, ids_ref, q_ref, own_ref, other_ref, num_ref, den_ref,
                 kv, num_acc, den_acc, list_b, list_r, sems):
     held = own_ref.shape[0]
     width = q_ref.shape[2]
@@ -124,19 +142,28 @@
     for copy in copies:
         copy.wait()
     ones = jnp.ones((8, kv.shape[1]), BF16)
-    for r in range(reads):
-        b, row = list_b[r], list_r[r]
-        for h in range(width // DV):
-            cols = slice(h * DV, (h + 1) * DV)
-            score = lax.dot_general(
-                q_ref[b, :, cols], kv[row, :, cols], NT, preferred_element_type=F32
-            )
-            expd = jnp.exp(score * (DV ** (-0.5))).astype(BF16)
-            num_acc[b, :, cols] += jnp.dot(
-                expd, kv[row, :, width + h * DV : width + (h + 1) * DV],
-                preferred_element_type=F32,
-            )
-            den_acc[h, b] += lax.dot_general(ones, expd, NT, preferred_element_type=F32)
+    group = 4 if reads % 4 == 0 else 1
+    heads = [(h, slice(h * DV, (h + 1) * DV)) for h in range(width // DV)]
+    for first in range(0, reads, group):
+        items = []
+        for r in range(first, first + group):
+            b, row = list_b[r], list_r[r]
+            for h, cols in heads:
+                score = lax.dot_general(
+                    q_ref[b, :, cols], kv[row, :, cols], NT, preferred_element_type=F32
+                )
+                items.append((b, row, h, cols, score))
+        exps = [jnp.exp(item[-1] * (DV ** (-0.5))).astype(BF16) for item in items]
+        made = []
+        for (b, row, h, cols, _), expd in zip(items, exps):
+            value = kv[row, :, width + h * DV : width + (h + 1) * DV]
+            made.append((
+                jnp.dot(expd, value, preferred_element_type=F32),
+                lax.dot_general(ones, expd, NT, preferred_element_type=F32),
+            ))
+        for (b, row, h, cols, _), (num, den) in zip(items, made):
+            num_acc[b, :, cols] += num
+            den_acc[h, b] += den
     num_ref[...] = num_acc[...].astype(BF16)
     for h in range(width // DV):
         for b in range(q_ref.shape[0]):
@@ -160,7 +187,7 @@
         for extra in dens[1:]:
             den = den + extra[h]
         inverse.append(jnp.transpose(1.0 / den, (1, 0)))
-    ones = jnp.ones((8, width), F32)
+    ones = jnp.ones((8, 2 * width), BF16)
     for b in range(blocks):
         rows = slice(b * BLK, (b + 1) * BLK)
         for h in range(heads):
@@ -172,7 +199,9 @@
                 gla_ref[rows, cols] + gate_ref[rows, cols] * (num * inverse[h][:, b : b + 1])
             )
         held = combined[rows, :]
-        sums = lax.dot_general(ones, held * held, NT, precision=PRECISE, preferred_element_type=F32)
+        sums = lax.dot_general(
+            ones, jnp.concatenate(split(held * held), axis=1), NT, preferred_element_type=F32
+        )
         mine[b : b + 1, :] = sums[0:1]
     pl.semaphore_wait(barrier, n_tp - 1)
     copies = []
@@ -213,6 +242,7 @@
     heads = width // DV
     stores_here, passage_rows, _ = store.shape
     tile = 2 * BLK
+    tall = 4 * BLK
     whole = lambda *shape: pl.BlockSpec(shape, lambda i, *_: (0,) * len(shape))
     any_spec = pl.BlockSpec(memory_space=pl.ANY)
     vmem = pl.BlockSpec(memory_space=pltpu.VMEM)
@@ -222,13 +252,13 @@
 
     read_query = pl.pallas_call(
         query_kernel,
-        grid=(length // tile,),
+        grid=(length // tall,),
         in_specs=[
-            pl.BlockSpec((tile, depth), lambda i: (i, 0)),
+            pl.BlockSpec((tall, depth), lambda i: (i, 0)),
             whole(depth, width),
             whole(1, DV),
         ],
-        out_specs=pl.BlockSpec((tile, width), lambda i: (i, 0)),
+        out_specs=pl.BlockSpec((tall, width), lambda i: (i, 0)),
         out_shape=jax.ShapeDtypeStruct((length, width), BF16),
         cost_estimate=cost(2 * length * depth * width, 6e6),
         name="query",
@@ -238,30 +268,31 @@
     queries = [read_query] + [shift(read_query, PAIR * k) for k in groups]
     ids = [passage_ids] + [shift(passage_ids, PAIR * k) for k in groups]
 
+    held_store, _ = lax.optimization_barrier((store, read_query))
     rows = stores_here * passage_rows
     made = pl.pallas_call(
         passage_kernel,
-        grid=(rows // tile,),
+        grid=(rows // tall,),
         in_specs=[
-            pl.BlockSpec((tile, depth), lambda i: (i, 0)),
+            pl.BlockSpec((tall, depth), lambda i: (i, 0)),
             whole(depth, width),
             whole(depth, width),
             whole(1, DV),
         ],
-        out_specs=pl.BlockSpec((tile, 2 * width), lambda i: (i, 0)),
+        out_specs=pl.BlockSpec((tall, 2 * width), lambda i: (i, 0)),
         out_shape=jax.ShapeDtypeStruct((rows, 2 * width), BF16),
         cost_estimate=cost(4 * rows * depth * width, 1e7),
         name="passages",
-    )(store.reshape(rows, depth), w_rkey, w_rvalue, key_gain.reshape(1, DV))
+    )(held_store.reshape(rows, depth), w_rkey, w_rvalue, key_gain.reshape(1, DV))
     made = made.reshape(stores_here, passage_rows, 2 * width)
     other = lax.ppermute(made, "st", [(s, s ^ 1) for s in range(n_st)])
 
     request_count = passage_ids.shape[0] * passage_ids.shape[1]
     most = request_count // min(n_st, request_count // 2)
-    nums, dens = [], []
-    for k, (query, names) in enumerate(zip(queries, ids)):
-        num, den = pl.pallas_call(
-            functools.partial(read_kernel, PAIR * most, n_st),
+
+    def read(names, query):
+        return pl.pallas_call(
+            functools.partial(read_kernel, PAIR * most),
             in_specs=[
                 pl.BlockSpec(memory_space=pltpu.SMEM), vmem, any_spec, any_spec,
             ],
@@ -281,10 +312,13 @@
             cost_estimate=cost(2e9, 5e6),
             name="reads",
         )(names, query, made, other)
-        if k:
-            num, den = shift(num, -PAIR * k), shift(den, -PAIR * k)
-        nums.append(num)
-        dens.append(den)
+
+    nums, dens = [], []
+    for k in groups:
+        num, den = read(ids[k], queries[k])
+        tokens, _ = lax.optimization_barrier((tokens, num))
+        nums.append(shift(num, -PAIR * k))
+        dens.append(shift(den, -PAIR * k))
 
     spare = -w_query.shape[1] % BLK
     if spare:
@@ -313,6 +347,11 @@
         name="gla",
     )(block_scale, tokens, decay_rate.reshape(1, dk), w_query, w_key, w_decay, w_value, w_gate)
 
+    read_query, gla_out = lax.optimization_barrier((read_query, gla_out))
+    num, den = read(passage_ids, read_query)
+    nums.append(num)
+    dens.append(den)
+
     return pl.pallas_call(
         functools.partial(finish_kernel, len(nums), n_tp),
         in_specs=[vmem] * (3 + 2 * len(nums)),
@@ -332,8 +371,11 @@
 
 
 def solution(mesh):
+    def body(*args):
+        return on_device(mesh.shape["st"], mesh.shape["tp"], *args)
+
     return jax.shard_map(
-        functools.partial(on_device, mesh.shape["st"], mesh.shape["tp"]),
+        body,
         mesh=mesh,
         in_specs=(
             P(("grp", "st"), None),

time: 81.3 us -> 68.3 us (0.84)
  Pallas kernels: 58.1 us -> 45.5 us
    pallas_call x4, Pallas kernels: 31.6 us -> 23.1 us  [the longest x2 11.4 us: read(): pl.pallas_call(functools.partial(read_kernel, PAIR * most), in_specs=[pl....]
    pallas_call x1, Pallas kernels: 16.7 us -> 13.1 us  [on_device(): pl.pallas_call(gla_kernel, grid=(length // tile,), in_specs=[pl.BlockSpec...]
  transfers between devices with their start and end apart: 5 -> 5, of which waited for: 1 -> 1; matrix products, arithmetic and copies ran while one was open for 0% -> 0% of each run, Pallas kernels for 38% -> 28%
where the time goes in v2:
time: 68.3 us; the launch traced here: 68 us
  Pallas kernels  45.5 us (67%)
  waiting for transfers between devices  12.5 us (18%)
  starting transfers between devices  5.18 us (8%)
  local copies, waits for them, and re-layouts  4.68 us (7%)
    pallas_call x1, Pallas kernels, on_device(): pl.pallas_call(gla_kernel, grid=(length // tile,), in_specs=[pl.BlockSpec...  13.1 us
    ppermute x4, waiting for transfers between devices, shift(): lax.ppermute(values, 'st', [(s, (s + by) % n_st) for s in range(n_st)])  12.5 us
    pallas_call x2, Pallas kernels, read(): pl.pallas_call(functools.partial(read_kernel, PAIR * most), in_specs=[pl....  11.4 us
    pallas_call x1, Pallas kernels, on_device(): pl.pallas_call(functools.partial(finish_kernel, len(nums), n_tp), in_spec...  9.27 us
    pallas_call x1, Pallas kernels, on_device(): pl.pallas_call(passage_kernel, grid=(rows // tall,), in_specs=[pl.BlockSp...  7.56 us
    ppermute x4, starting transfers between devices, shift(): lax.ppermute(values, 'st', [(s, (s + by) % n_st) for s in range(n_st)])  4.69 us
    unnamed x18, local copies, waits for them, and re-layouts  4.68 us
    pallas_call x1, Pallas kernels, on_device(): pl.pallas_call(query_kernel, grid=(length // tall,), in_specs=[pl.BlockSp...  4.19 us
  transfers between devices with their start and end apart: 5, of which 1 were waited for; matrix products, arithmetic and copies ran while one was open for 0% of the time, Pallas kernels for 28%

profile of v2, /device:TPU:0, one launch (start us, length us, event | category | flops | bytes accessed | tf_op | source)
XLA Modules:
  0.0 68.0 jit_solution(3362556650571075453)
XLA Ops:
  0.0 4.2 %query.1 = bf16[1024,256]{1,0:T(8,128)(2,1)} custom-call(bf16[1024,2048]{1,0:T(8,128)(2,1)} %tok_ref.2, bf16[2048,256]{1,0:T(8,128)(2,1)} %w_ref.1, f32[1,128]{1,0:T(1,128)} %bitcast.9), custom_call_target="tpu_custom_call" | custom-call | flops 1073741824 | bytes 6000000 | tf_op jit(solution)/shard_map/query/pallas_call | solution.py:253
  4.2 0.0 copy-start
  4.2 0.0 copy-start.2
  4.2 7.6 %passages.1 = bf16[1536,512]{1,0:T(8,128)(2,1)} custom-call(bf16[1536,2048]{1,0:T(8,128)(2,1)} %bitcast.10, bf16[2048,256]{1,0:T(8,128)(2,1)} %wk_ref.1, bf16[2048,256]{1,0:T(8,128)(2,1)} %wv_ref.1, f32[1,128]{1,0:T(1,128)} %bitcast.15), custom_call_target="tpu_custom_call" | custom-call | flops 3221225472 | bytes 10000000 | tf_op jit(solution)/shard_map/passages/pallas_call | solution.py:273
  11.8 0.5 collective-permute-start.2
  12.3 0.0 copy-done
  12.3 2.6 %collective-permute-start.1 = (bf16[8,128,256]{2,1,0:T(8,128)(2,1)S(1)}, bf16[8,128,256]{2,1,0:T(8,128)(2,1)S(1)}, u32[]{:S(2)}, u32[]{:S(2)}) collective-permute-start(bf16[8,128,256]{2,1,0:T(8,128)(2,1)S(1)} %bitcast.8), channel_id=1, source_target_pairs={{0,8},{4,12},{8,0},{12,4},{1,9},{5,13},{9,1},{13,5},{2,10},{6,14},... | collective-permute-start | bytes 1572872 | tf_op jit(solution)/shard_map/ppermute | solution.py:251
  14.8 0.0 copy-done.2
  14.8 0.1 copy.17.ids_ref
  14.9 0.0 copy-start.1
  14.9 0.0 collective-permute-start
  14.9 12.5 %collective-permute-done.ids_ref = s32[8,4]{1,0:T(8,128)S(1)} collective-permute-done((s32[8,4]{1,0:T(8,128)S(1)}, s32[8,4]{1,0:T(8,128)S(1)}, u32[]{:S(2)}, u32[]{:S(2)}) %collective-permute-start) | collective-permute-done | bytes 160 | tf_op jit(solution)/shard_map/ppermute | solution.py:251
  27.4 0.0 copy-start.7
  27.4 0.0 collective-permute-done.1.q_ref
  27.4 0.0 copy-start.5
  27.4 0.0 collective-permute-done.2.other_ref
  27.5 0.6 copy-done.7
  28.0 0.2 copy-done.5
  28.2 0.0 copy-start.3
  28.3 1.1 %copy-done.3 = bf16[12,128,512]{2,1,0:T(8,128)(2,1)} copy-done((bf16[12,128,512]{2,1,0:T(8,128)(2,1)}, bf16[12,128,512]{2,1,0:T(8,128)(2,1)S(1)}, u32[]{:S(2)}) %copy-start.3) | copy-done | bytes 1572888
  29.4 5.7 %reads.2 = (bf16[8,128,256]{2,1,0:T(8,128)(2,1)}, f32[2,8,128]{2,1,0:T(8,128)}) custom-call(s32[8,4]{1,0:T(8,128)} %copy-done.7, bf16[8,128,256]{2,1,0:T(8,128)(2,1)} %copy-done.5, bf16[12,128,512]{2,1,0:T(8,128)(2,1)} %bitcast.12, bf16[12,128,512]{2,1,0:T(8,128)(2,1)} %copy-done.3), custom_call_target="tpu_custom_call" | custom-call | flops 2000000000 | bytes 5000000 | tf_op jit(solution)/shard_map/reads/pallas_call | solution.py:294
  35.1 1.8 %collective-permute-start.3 = (bf16[8,128,256]{2,1,0:T(8,128)(2,1)}, bf16[8,128,256]{2,1,0:T(8,128)(2,1)S(1)}, u32[]{:S(2)}, u32[]{:S(2)}) collective-permute-start(bf16[8,128,256]{2,1,0:T(8,128)(2,1)} %get-tuple-element.16), channel_id=1, source_target_pairs={{0,8},{4,12},{8,0},{12,4},{1,9},{5,13},{9,1},{13,5},{2,10},{6,14},... | collective-permute-start | bytes 1572872 | tf_op jit(solution)/shard_map/ppermute | solution.py:251
  36.9 0.3 collective-permute-start.4
  37.2 13.1 %gla.1 = (f32[1024,256]{1,0:T(8,128)}, f32[1024,256]{1,0:T(8,128)}) custom-call(f32[8]{0:T(128)} %scale_ref.1, bf16[1024,2048]{1,0:T(8,128)(2,1)} %tok_ref.2, f32[1,128]{1,0:T(1,128)} %bitcast.16, bf16[2048,128]{1,0:T(8,128)(2,1)} %wq.1, bf16[2048,128]{1,0:T(8,128)(2,1)} %wk.1, bf16[2048,128]{1,0:T(8,128)(2,1)} %wd.1, bf16[2048,256]{1,0:T(8,128)(2,1)} %wv.1, ...), custom_call_target="tpu_custom_call" | custom-call | flops 8000000000 | bytes 10000000 | tf_op jit(solution)/shard_map/gla/pallas_call | solution.py:330
  50.3 0.0 copy-done.1
  50.3 5.7 %reads.3 = (bf16[8,128,256]{2,1,0:T(8,128)(2,1)}, f32[2,8,128]{2,1,0:T(8,128)}) custom-call(s32[8,4]{1,0:T(8,128)} %copy-done.1, bf16[8,128,256]{2,1,0:T(8,128)(2,1)} %bitcast.7, bf16[12,128,512]{2,1,0:T(8,128)(2,1)} %bitcast.13, bf16[12,128,512]{2,1,0:T(8,128)(2,1)} %copy-done.3), custom_call_target="tpu_custom_call" | custom-call | flops 2000000000 | bytes 5000000 | tf_op jit(solution)/shard_map/reads/pallas_call | solution.py:294
  56.0 0.0 collective-permute-done.4.refs_5_
  56.0 0.0 copy-start.6
  56.0 0.0 collective-permute-done.3.refs_3_
  56.0 0.0 copy-start.4
  56.0 0.6 copy-done.6
  56.6 0.2 copy-done.4
  56.8 9.3 %finish.1 = bf16[1024,256]{1,0:T(8,128)(2,1)} custom-call(f32[1024,256]{1,0:T(8,128)} %get-tuple-element.19.refs_0_, f32[1024,256]{1,0:T(8,128)} %get-tuple-element.20.refs_1_, f32[1,256]{1,0:T(1,128)} %bitcast.14, bf16[8,128,256]{2,1,0:T(8,128)(2,1)} %copy-done.4, bf16[8,128,256]{2,1,0:T(8,128)(2,1)} %get-tuple-element.22.refs_4_, f32[2,8,128]{2,1,0:T(8,128)} %copy-done.6, ...), custom_call_target="tpu_custom_call" | custom-call | flops 1000000000 | bytes 6000000 | tf_op jit(solution)/shard_map/finish/pallas_call | solution.py:355
  66.1 1.9 %copy.20 = bf16[1024,256]{1,0:T(8,128)(2,1)} copy(bf16[1024,256]{1,0:T(8,128)(2,1)} %finish.1) | data formatting | bytes 1048576
Async XLA Ops:
  4.2 8.1 %copy-start = (bf16[1024,256]{1,0:T(8,128)(2,1)S(1)}, bf16[1024,256]{1,0:T(8,128)(2,1)}, u32[]{:S(2)}) copy-start(bf16[1024,256]{1,0:T(8,128)(2,1)} %query.1) | copy-start | bytes 1572868
  4.2 10.6 %copy-start.2 = (s32[8,4]{0,1:T(4,128)S(1)}, s32[8,4]{0,1:T(4,128)}, u32[]{:S(2)}) copy-start(s32[8,4]{0,1:T(4,128)} %param.31) | copy-start | bytes 388
  11.8 15.7 %collective-permute-start.2 = (bf16[12,128,512]{2,1,0:T(8,128)(2,1)}, bf16[12,128,512]{2,1,0:T(8,128)(2,1)S(1)}, u32[]{:S(2)}, u32[]{:S(2)}) collective-permute-start(bf16[12,128,512]{2,1,0:T(8,128)(2,1)} %bitcast.11), channel_id=1, source_target_pairs={{0,4},{4,0},{8,12},{12,8},{1,5},{5,1},{9,13},{13,9},{2,6},{6,2},{1... | collective-permute-start | bytes 4718600 | tf_op jit(solution)/shard_map/ppermute | solution.py:288
  12.3 15.2 %collective-permute-start.1 = (bf16[8,128,256]{2,1,0:T(8,128)(2,1)S(1)}, bf16[8,128,256]{2,1,0:T(8,128)(2,1)S(1)}, u32[]{:S(2)}, u32[]{:S(2)}) collective-permute-start(bf16[8,128,256]{2,1,0:T(8,128)(2,1)S(1)} %bitcast.8), channel_id=1, source_target_pairs={{0,8},{4,12},{8,0},{12,4},{1,9},{5,13},{9,1},{13,5},{2,10},{6,14},... | collective-permute-start | bytes 1572872 | tf_op jit(solution)/shard_map/ppermute | solution.py:251
  14.9 35.4 %copy-start.1 = (s32[8,4]{1,0:T(8,128)}, s32[8,4]{1,0:T(8,128)S(1)}, u32[]{:S(2)}) copy-start(s32[8,4]{1,0:T(8,128)S(1)} %copy.17.ids_ref) | copy-start | bytes 388
  14.9 12.5 %collective-permute-start = (s32[8,4]{1,0:T(8,128)S(1)}, s32[8,4]{1,0:T(8,128)S(1)}, u32[]{:S(2)}, u32[]{:S(2)}) collective-permute-start(s32[8,4]{1,0:T(8,128)S(1)} %copy.17.ids_ref), channel_id=1, source_target_pairs={{0,8},{4,12},{8,0},{12,4},{1,9},{5,13},{9,1},{13,5},{2,10},{6,14},... | collective-permute-start | bytes 392 | tf_op jit(solution)/shard_map/ppermute | solution.py:251
  27.4 0.6 copy-start.7
  27.4 0.8 %copy-start.5 = (bf16[8,128,256]{2,1,0:T(8,128)(2,1)}, bf16[8,128,256]{2,1,0:T(8,128)(2,1)S(1)}, u32[]{:S(2)}) copy-start(bf16[8,128,256]{2,1,0:T(8,128)(2,1)S(1)} %collective-permute-done.1.q_ref) | copy-start | bytes 1572868
  28.2 1.1 %copy-start.3 = (bf16[12,128,512]{2,1,0:T(8,128)(2,1)}, bf16[12,128,512]{2,1,0:T(8,128)(2,1)S(1)}, u32[]{:S(2)}) copy-start(bf16[12,128,512]{2,1,0:T(8,128)(2,1)S(1)} %collective-permute-done.2.other_ref) | copy-start | bytes 4718596
  35.1 20.9 %collective-permute-start.3 = (bf16[8,128,256]{2,1,0:T(8,128)(2,1)}, bf16[8,128,256]{2,1,0:T(8,128)(2,1)S(1)}, u32[]{:S(2)}, u32[]{:S(2)}) collective-permute-start(bf16[8,128,256]{2,1,0:T(8,128)(2,1)} %get-tuple-element.16), channel_id=1, source_target_pairs={{0,8},{4,12},{8,0},{12,4},{1,9},{5,13},{9,1},{13,5},{2,10},{6,14},... | collective-permute-start | bytes 1572872 | tf_op jit(solution)/shard_map/ppermute | solution.py:251
  36.9 19.1 %collective-permute-start.4 = (f32[2,8,128]{2,1,0:T(8,128)}, f32[2,8,128]{2,1,0:T(8,128)S(1)}, u32[]{:S(2)}, u32[]{:S(2)}) collective-permute-start(f32[2,8,128]{2,1,0:T(8,128)} %get-tuple-element.23), channel_id=1, source_target_pairs={{0,8},{4,12},{8,0},{12,4},{1,9},{5,13},{9,1},{13,5},{2,10},{6,14},... | collective-permute-start | bytes 24584 | tf_op jit(solution)/shard_map/ppermute | solution.py:251
  56.0 0.6 copy-start.6
  56.0 0.8 %copy-start.4 = (bf16[8,128,256]{2,1,0:T(8,128)(2,1)}, bf16[8,128,256]{2,1,0:T(8,128)(2,1)S(1)}, u32[]{:S(2)}) copy-start(bf16[8,128,256]{2,1,0:T(8,128)(2,1)S(1)} %collective-permute-done.3.refs_3_) | copy-start | bytes 1572868

commit v3 on v2

--- a/solution.py
+++ b/solution.py
@@ -48,7 +48,8 @@
 
 
 def gla_kernel(
-    scale_ref, tok_ref, rate_ref, wq, wk, wd, wv, wg, gla_ref, gate_ref, w_all, state, sems
+    first, scale_ref, tok_ref, rate_ref, given, wq, wk, wd, wv, wg,
+    gla_ref, gate_ref, kept, w_all, state, sems
 ):
     step = pl.program_id(0)
     dk = wq.shape[1]
@@ -65,7 +66,7 @@
             at += w.shape[1]
         for copy in copies:
             copy.start()
-        state[...] = jnp.zeros_like(state)
+        state[...] = given[...]
         for copy in copies:
             copy.wait()
 
@@ -77,43 +78,72 @@
     lower = causal.astype(F32)
     lower = jnp.concatenate([lower, lower], axis=1).astype(BF16)
     lane_head = lax.broadcasted_iota(jnp.int32, (BLK, dk), 1) // DK
+    zero = jnp.zeros((), BF16)
     blocks = tok_ref.shape[0] // BLK
+    spans = [slice(i * BLK, (i + 1) * BLK) for i in range(blocks)]
+    heads = [slice(h * DV, (h + 1) * DV) for h in range(dv // DV)]
+    cums = []
+    for i, rows in enumerate(spans):
+        pre = made[rows, 2 * dk : 3 * dk]
+        block_scale = scale_ref[first + step * blocks + i]
+        high, low = split(-2.0 * rate_ref[...] * jax.nn.sigmoid(pre) * block_scale)
+        cums.append(
+            jnp.dot(lower, jnp.concatenate([high, low], axis=0), preferred_element_type=F32)
+        )
+    queries, scores, ups, totals, values = [], [], [], [], []
+    for rows, cum in zip(spans, cums):
+        q, k = made[rows, :dk], made[rows, dk : 2 * dk]
+        total = cum[BLK - 1 : BLK, :]
+        totals.append(jnp.exp(total))
+        q_high, q_low = split(q * (DK ** (-0.5)) * jnp.exp(cum))
+        k_high, k_low = split(k * jnp.exp(-cum))
+        k_twice = jnp.concatenate([k_high, k_high], axis=1)
+        ups.append(split(k * jnp.exp(total - cum)))
+        values.append(split(made[rows, 3 * dk : 3 * dk + dv]))
+        for h in range(len(heads)):
+            own_high = jnp.where(lane_head == h, q_high, zero)
+            own_low = jnp.where(lane_head == h, q_low, zero)
+            q_h = jnp.concatenate([own_high, own_low], axis=1)
+            queries.append(q_h)
+            scores.append(
+                lax.dot_general(q_h, k_twice, NT, preferred_element_type=F32)
+                + lax.dot_general(own_high, k_low, NT, preferred_element_type=F32)
+            )
+    within, added = [], []
     for i in range(blocks):
-        rows = slice(i * BLK, (i + 1) * BLK)
-        q, k = made[rows, :dk], made[rows, dk : 2 * dk]
-        pre, v = made[rows, 2 * dk : 3 * dk], made[rows, 3 * dk : 3 * dk + dv]
-        block_scale = scale_ref[step * blocks + i]
-        log_decay = -2.0 * rate_ref[...] * jax.nn.sigmoid(pre) * block_scale
-        high, low = split(log_decay)
-        cum = jnp.dot(
-            lower, jnp.concatenate([high, low], axis=0), preferred_element_type=F32
-        )
-        total = cum[BLK - 1 : BLK, :]
-        k_dec = k * jnp.exp(-cum)
-        q_high, q_low = split(q * (DK ** (-0.5)) * jnp.exp(cum))
-        k_high, k_low = split(k_dec)
-        k_twice = jnp.concatenate([k_high, k_high], axis=1)
-        up = jnp.concatenate(split(k * jnp.exp(total - cum)), axis=1)
-        v_high = v.astype(BF16)
+        v_high, v_low = values[i]
         v_twice = jnp.concatenate([v_high, v_high], axis=0)
-        held = state[...]
+        for h, cols in enumerate(heads):
+            high, low = split(jnp.where(causal, scores[i * len(heads) + h], 0.0))
+            within.append(
+                jnp.dot(
+                    jnp.concatenate([high, low], axis=1),
+                    v_twice[:, cols],
+                    preferred_element_type=F32,
+                )
+                + jnp.dot(high, v_low[:, cols], preferred_element_type=F32)
+            )
+        up_high, up_low = ups[i]
+        both = lax.dot_general(
+            v_high, jnp.concatenate([up_high, up_low], axis=1), TN, preferred_element_type=F32
+        )
+        added.append(
+            both[:, :dk]
+            + both[:, dk:]
+            + lax.dot_general(v_low, up_high, TN, preferred_element_type=F32)
+        )
+    held = state[...]
+    for i, rows in enumerate(spans):
         held_high = held.astype(BF16)
         held_twice = jnp.concatenate([held_high, held_high], axis=1)
-        for h in range(dv // DV):
-            cols = slice(h * DV, (h + 1) * DV)
-            mine = lane_head == h
-            zero = jnp.zeros((), BF16)
-            own_high = jnp.where(mine, q_high, zero)
-            q_h = jnp.concatenate([own_high, jnp.where(mine, q_low, zero)], axis=1)
-            scores = lax.dot_general(
-                q_h, k_twice, NT, preferred_element_type=F32
-            ) + lax.dot_general(own_high, k_low, NT, preferred_element_type=F32)
-            scores = jnp.concatenate(split(jnp.where(causal, scores, 0.0)), axis=1)
-            gla_ref[rows, cols] = jnp.dot(
-                scores, v_twice[:, cols], preferred_element_type=F32
-            ) + lax.dot_general(q_h, held_twice[cols], NT, preferred_element_type=F32)
-        added = lax.dot_general(v_high, up, TN, preferred_element_type=F32)
-        state[...] = held * jnp.exp(total) + added[:, :dk] + added[:, dk:]
+        for h, cols in enumerate(heads):
+            n = i * len(heads) + h
+            gla_ref[rows, cols] = within[n] + lax.dot_general(
+                queries[n], held_twice[cols], NT, preferred_element_type=F32
+            )
+        held = held * totals[i] + added[i]
+    state[...] = held
+    kept[...] = held
 
 
 def read_kernel(reads, ids_ref, q_ref, own_ref, other_ref, num_ref, den_ref,
@@ -171,15 +201,31 @@
 
 
 def finish_kernel(parts, n_tp, *refs):
-    gla_ref, gate_ref, gain_ref = refs[:3]
-    nums, dens = refs[3 : 3 + parts], refs[3 + parts : 3 + 2 * parts]
-    out_ref, combined, mine, theirs, send_sems, recv_sems = refs[3 + 2 * parts :]
+    gain_ref, gla_parts, gate_parts = refs[0], refs[1:3], refs[3:5]
+    refs = refs[5:]
+    far, dens = refs[:parts], refs[parts : 2 * parts]
+    (out_ref, gla_ref, gate_ref, *nums) = refs[2 * parts : 3 * parts + 3]
+    combined, mine, theirs, send_sems, recv_sems, sems = refs[3 * parts + 3 :]
+    blocks = mine.shape[0]
+    half = blocks // 2
+    loads = []
+    for b in range(blocks):
+        there, here = pl.ds(b % half * BLK, BLK), pl.ds(b * BLK, BLK)
+        row = [
+            pltpu.make_async_copy(gla_parts[b // half].at[there], gla_ref.at[here], sems.at[0, b]),
+            pltpu.make_async_copy(gate_parts[b // half].at[there], gate_ref.at[here], sems.at[1, b]),
+        ]
+        for i in range(parts):
+            row.append(pltpu.make_async_copy(far[i].at[b], nums[i].at[b], sems.at[2 + i, b]))
+        for copy in row:
+            copy.start()
+        loads.append(row)
     me = lax.axis_index("tp")
     barrier = pltpu.get_barrier_semaphore()
     peers = [lax.rem(me + k, n_tp) for k in range(1, n_tp)]
     for peer in peers:
         pl.semaphore_signal(barrier, inc=1, device_id={"tp": peer}, device_id_type=MESH)
-    blocks, heads = mine.shape[0], dens[0].shape[0]
+    heads = dens[0].shape[0]
     width = out_ref.shape[1]
     inverse = []
     for h in range(heads):
@@ -190,6 +236,8 @@
     ones = jnp.ones((8, 2 * width), BF16)
     for b in range(blocks):
         rows = slice(b * BLK, (b + 1) * BLK)
+        for copy in loads[b]:
+            copy.wait()
         for h in range(heads):
             cols = slice(h * DV, (h + 1) * DV)
             num = nums[0][b, :, cols].astype(F32)
@@ -286,6 +334,43 @@
     )(held_store.reshape(rows, depth), w_rkey, w_rvalue, key_gain.reshape(1, DV))
     made = made.reshape(stores_here, passage_rows, 2 * width)
     other = lax.ppermute(made, "st", [(s, s ^ 1) for s in range(n_st)])
+
+    spare = -w_query.shape[1] % BLK
+    if spare:
+        w_query, w_key, w_decay = (
+            jnp.pad(w, ((0, 0), (0, spare))) for w in (w_query, w_key, w_decay)
+        )
+        decay_rate = jnp.pad(decay_rate, (0, spare))
+    dk = w_query.shape[1]
+    half = length // 2
+
+    def linear(first, values, state):
+        return pl.pallas_call(
+            functools.partial(gla_kernel, first // BLK),
+            grid=(half // tile,),
+            in_specs=[
+                pl.BlockSpec(memory_space=pltpu.SMEM),
+                pl.BlockSpec((tile, depth), lambda i: (i + first // tile, 0)),
+                whole(1, dk),
+                whole(width, dk),
+            ]
+            + [any_spec] * 5,
+            out_specs=[pl.BlockSpec((tile, width), lambda i: (i, 0))] * 2 + [whole(width, dk)],
+            out_shape=[jax.ShapeDtypeStruct((half, width), F32)] * 2
+            + [jax.ShapeDtypeStruct((width, dk), F32)],
+            scratch_shapes=[
+                pltpu.VMEM((depth, 3 * dk + 2 * width), BF16),
+                pltpu.VMEM((width, dk), F32),
+                pltpu.SemaphoreType.DMA((5,)),
+            ],
+            cost_estimate=cost(4e9, 7e6),
+            name="gla",
+        )(block_scale, values, decay_rate.reshape(1, dk), state,
+          w_query, w_key, w_decay, w_value, w_gate)
+
+    early_tokens, _ = lax.optimization_barrier((tokens, made))
+    gla_first, gate_first, state = linear(0, early_tokens, jnp.zeros((width, dk), F32))
+    made, _ = lax.optimization_barrier((made, gla_first))
 
     request_count = passage_ids.shape[0] * passage_ids.shape[1]
     most = request_count // min(n_st, request_count // 2)
@@ -320,33 +405,7 @@
         nums.append(shift(num, -PAIR * k))
         dens.append(shift(den, -PAIR * k))
 
-    spare = -w_query.shape[1] % BLK
-    if spare:
-        w_query, w_key, w_decay = (
-            jnp.pad(w, ((0, 0), (0, spare))) for w in (w_query, w_key, w_decay)
-        )
-        decay_rate = jnp.pad(decay_rate, (0, spare))
-    dk = w_query.shape[1]
-    gla_out, gate = pl.pallas_call(
-        gla_kernel,
-        grid=(length // tile,),
-        in_specs=[
-            pl.BlockSpec(memory_space=pltpu.SMEM),
-            pl.BlockSpec((tile, depth), lambda i: (i, 0)),
-            whole(1, dk),
-        ]
-        + [any_spec] * 5,
-        out_specs=[pl.BlockSpec((tile, width), lambda i: (i, 0))] * 2,
-        out_shape=[jax.ShapeDtypeStruct((length, width), F32)] * 2,
-        scratch_shapes=[
-            pltpu.VMEM((depth, 3 * dk + 2 * width), BF16),
-            pltpu.VMEM((width, dk), F32),
-            pltpu.SemaphoreType.DMA((5,)),
-        ],
-        cost_estimate=cost(8e9, 1e7),
-        name="gla",
-    )(block_scale, tokens, decay_rate.reshape(1, dk), w_query, w_key, w_decay, w_value, w_gate)
-
+    gla_out, gate, _ = linear(half, tokens, state)
     read_query, gla_out = lax.optimization_barrier((read_query, gla_out))
     num, den = read(passage_ids, read_query)
     nums.append(num)
@@ -354,20 +413,23 @@
 
     return pl.pallas_call(
         functools.partial(finish_kernel, len(nums), n_tp),
-        in_specs=[vmem] * (3 + 2 * len(nums)),
+        in_specs=[vmem] + [any_spec] * (4 + len(nums)) + [vmem] * len(nums),
         out_specs=vmem,
         out_shape=jax.ShapeDtypeStruct((length, width), BF16),
-        scratch_shapes=[
+        scratch_shapes=[pltpu.VMEM((length, width), F32)] * 2
+        + [pltpu.VMEM((num_blocks, BLK, width), BF16)] * len(nums)
+        + [
             pltpu.VMEM((length, width), F32),
             pltpu.VMEM((num_blocks, BLK), F32),
             pltpu.VMEM((max(n_tp - 1, 1), num_blocks, BLK), F32),
             pltpu.SemaphoreType.DMA((max(n_tp - 1, 1),)),
             pltpu.SemaphoreType.DMA((max(n_tp - 1, 1),)),
+            pltpu.SemaphoreType.DMA((2 + len(nums), num_blocks)),
         ],
         compiler_params=pltpu.CompilerParams(collective_id=0, has_side_effects=True),
         cost_estimate=cost(1e9, 6e6),
         name="finish",
-    )(gla_out, gate, out_gain.reshape(1, width), *nums, *dens)
+    )(out_gain.reshape(1, width), gla_first, gla_out, gate_first, gate, *nums, *dens)
 
 
 def solution(mesh):

time: 68.3 us -> 64.6 us (0.946)
  waiting for transfers between devices: 12.5 us -> 3.94 us
  Pallas kernels: 45.5 us -> 49.7 us
  local copies, waits for them, and re-layouts: 4.68 us -> 5.37 us
    ppermute x4, waiting for transfers between devices: 12.5 us -> 3.94 us  [shift(): lax.ppermute(values, 'st', [(s, (s + by) % n_st) for s in range(n_st)])]
    pallas_call x1 -> x2, Pallas kernels: 13.1 us -> 15.8 us  [linear(): pl.pallas_call(functools.partial(gla_kernel, first // BLK), grid=(half //...]
    pallas_call x1, Pallas kernels: 9.27 us -> 10.7 us  [on_device(): pl.pallas_call(functools.partial(finish_kernel, len(nums), n_tp), in_spec...]
  transfers between devices with their start and end apart: 5 -> 5, of which waited for: 1 -> 1; matrix products, arithmetic and copies ran while one was open for 0% -> 1% of each run, Pallas kernels for 28% -> 33%
where the time goes in v3:
time: 64.6 us; the launch traced here: 64.3 us
  Pallas kernels  49.7 us (77%)
  local copies, waits for them, and re-layouts  5.37 us (8%)
  starting transfers between devices  5.18 us (8%)
  waiting for transfers between devices  3.94 us (6%)
    pallas_call x2, Pallas kernels, linear(): pl.pallas_call(functools.partial(gla_kernel, first // BLK), grid=(half //...  15.8 us
    pallas_call x2, Pallas kernels, read(): pl.pallas_call(functools.partial(read_kernel, PAIR * most), in_specs=[pl....  11.4 us
    pallas_call x1, Pallas kernels, on_device(): pl.pallas_call(functools.partial(finish_kernel, len(nums), n_tp), in_spec...  10.7 us
    pallas_call x1, Pallas kernels, on_device(): pl.pallas_call(passage_kernel, grid=(rows // tall,), in_specs=[pl.BlockSp...  7.56 us
    unnamed x18, local copies, waits for them, and re-layouts  4.71 us
    ppermute x4, starting transfers between devices, shift(): lax.ppermute(values, 'st', [(s, (s + by) % n_st) for s in range(n_st)])  4.69 us
    pallas_call x1, Pallas kernels, on_device(): pl.pallas_call(query_kernel, grid=(length // tall,), in_specs=[pl.BlockSp...  4.18 us
    ppermute x4, waiting for transfers between devices, shift(): lax.ppermute(values, 'st', [(s, (s + by) % n_st) for s in range(n_st)])  3.94 us
  transfers between devices with their start and end apart: 5, of which 1 were waited for; matrix products, arithmetic and copies ran while one was open for 1% of the time, Pallas kernels for 33%

profile of v3, /device:TPU:0, one launch (start us, length us, event | category | flops | bytes accessed | tf_op | source)
XLA Modules:
  0.0 64.3 jit_solution(15429071325980766528)
XLA Ops:
  0.0 4.2 %query.1 = bf16[1024,256]{1,0:T(8,128)(2,1)} custom-call(bf16[1024,2048]{1,0:T(8,128)(2,1)} %tok_ref.3, bf16[2048,256]{1,0:T(8,128)(2,1)} %w_ref.1, f32[1,128]{1,0:T(1,128)} %bitcast.9), custom_call_target="tpu_custom_call" | custom-call | flops 1073741824 | bytes 6000000 | tf_op jit(solution)/shard_map/query/pallas_call | solution.py:301
  4.2 0.0 copy-start
  4.2 0.0 copy-start.2
  4.2 7.6 %passages.1 = bf16[1536,512]{1,0:T(8,128)(2,1)} custom-call(bf16[1536,2048]{1,0:T(8,128)(2,1)} %bitcast.10, bf16[2048,256]{1,0:T(8,128)(2,1)} %wk_ref.1, bf16[2048,256]{1,0:T(8,128)(2,1)} %wv_ref.1, f32[1,128]{1,0:T(1,128)} %bitcast.15), custom_call_target="tpu_custom_call" | custom-call | flops 3221225472 | bytes 10000000 | tf_op jit(solution)/shard_map/passages/pallas_call | solution.py:321
  11.7 0.5 collective-permute-start.2
  12.2 0.0 copy-done
  12.2 2.6 %collective-permute-start.1 = (bf16[8,128,256]{2,1,0:T(8,128)(2,1)S(1)}, bf16[8,128,256]{2,1,0:T(8,128)(2,1)S(1)}, u32[]{:S(2)}, u32[]{:S(2)}) collective-permute-start(bf16[8,128,256]{2,1,0:T(8,128)(2,1)S(1)} %bitcast.8), channel_id=1, source_target_pairs={{0,8},{4,12},{8,0},{12,4},{1,9},{5,13},{9,1},{13,5},{2,10},{6,14},... | collective-permute-start | bytes 1572872 | tf_op jit(solution)/shard_map/ppermute | solution.py:299
  14.8 0.0 copy-done.2
  14.8 0.1 copy.17.ids_ref
  14.9 0.0 copy-start.1
  14.9 0.0 collective-permute-start
  14.9 0.7 %broadcast_in_dim.3.given = f32[256,128]{1,0:T(8,128)} broadcast(f32[]{:T(128)} %constant.0.clone.1), dimensions={} | broadcast | bytes 131076 | tf_op jit(solution)/shard_map/broadcast_in_dim | solution.py:372
  15.6 7.9 %gla.2 = (f32[512,256]{1,0:T(8,128)}, f32[512,256]{1,0:T(8,128)}, f32[256,128]{1,0:T(8,128)}) custom-call(f32[8]{0:T(128)} %scale_ref.3, bf16[1024,2048]{1,0:T(8,128)(2,1)} %tok_ref.3, f32[1,128]{1,0:T(1,128)} %bitcast.16, f32[256,128]{1,0:T(8,128)} %broadcast_in_dim.3.given, bf16[2048,128]{1,0:T(8,128)(2,1)} %wq.3, bf16[2048,128]{1,0:T(8,128)(2,1)} %wk.3, ...), custom_call_target="tpu_custom_call" | custom-call | flops 4000000000 | bytes 7000000 | tf_op jit(solution)/shard_map/gla/pallas_call | solution.py:348
  23.5 0.0 copy-done.1
  23.5 3.9 %collective-permute-done.ids_ref = s32[8,4]{1,0:T(8,128)S(1)} collective-permute-done((s32[8,4]{1,0:T(8,128)S(1)}, s32[8,4]{1,0:T(8,128)S(1)}, u32[]{:S(2)}, u32[]{:S(2)}) %collective-permute-start) | collective-permute-done | bytes 160 | tf_op jit(solution)/shard_map/ppermute | solution.py:299
  27.4 0.0 copy-start.7
  27.4 0.0 collective-permute-done.1.q_ref
  27.4 0.0 copy-start.5
  27.4 0.0 collective-permute-done.2.other_ref
  27.4 0.6 copy-done.7
  28.0 0.2 copy-done.5
  28.2 0.0 copy-start.3
  28.2 1.1 %copy-done.3 = bf16[12,128,512]{2,1,0:T(8,128)(2,1)} copy-done((bf16[12,128,512]{2,1,0:T(8,128)(2,1)}, bf16[12,128,512]{2,1,0:T(8,128)(2,1)S(1)}, u32[]{:S(2)}) %copy-start.3) | copy-done | bytes 1572888
  29.4 5.7 %reads.2 = (bf16[8,128,256]{2,1,0:T(8,128)(2,1)}, f32[2,8,128]{2,1,0:T(8,128)}) custom-call(s32[8,4]{1,0:T(8,128)} %copy-done.7, bf16[8,128,256]{2,1,0:T(8,128)(2,1)} %copy-done.5, bf16[12,128,512]{2,1,0:T(8,128)(2,1)} %bitcast.12, bf16[12,128,512]{2,1,0:T(8,128)(2,1)} %copy-done.3), custom_call_target="tpu_custom_call" | custom-call | flops 2000000000 | bytes 5000000 | tf_op jit(solution)/shard_map/reads/pallas_call | solution.py:379
  35.1 1.8 %collective-permute-start.3 = (bf16[8,128,256]{2,1,0:T(8,128)(2,1)}, bf16[8,128,256]{2,1,0:T(8,128)(2,1)S(1)}, u32[]{:S(2)}, u32[]{:S(2)}) collective-permute-start(bf16[8,128,256]{2,1,0:T(8,128)(2,1)} %get-tuple-element.24), channel_id=1, source_target_pairs={{0,8},{4,12},{8,0},{12,4},{1,9},{5,13},{9,1},{13,5},{2,10},{6,14},... | collective-permute-start | bytes 1572872 | tf_op jit(solution)/shard_map/ppermute | solution.py:299
  36.9 0.3 collective-permute-start.4
  37.2 7.9 %gla.3 = (f32[512,256]{1,0:T(8,128)}, f32[512,256]{1,0:T(8,128)}, f32[256,128]{1,0:T(8,128)}) custom-call(f32[8]{0:T(128)} %scale_ref.3, bf16[1024,2048]{1,0:T(8,128)(2,1)} %tok_ref.3, f32[1,128]{1,0:T(1,128)} %bitcast.17, f32[256,128]{1,0:T(8,128)} %get-tuple-element.26.given, bf16[2048,128]{1,0:T(8,128)(2,1)} %wq.3, bf16[2048,128]{1,0:T(8,128)(2,1)} %wk.3, ...), custom_call_target="tpu_custom_call" | custom-call | flops 4000000000 | bytes 7000000 | tf_op jit(solution)/shard_map/gla/pallas_call | solution.py:348
  45.1 5.7 %reads.3 = (bf16[8,128,256]{2,1,0:T(8,128)(2,1)}, f32[2,8,128]{2,1,0:T(8,128)}) custom-call(s32[8,4]{1,0:T(8,128)} %copy-done.1, bf16[8,128,256]{2,1,0:T(8,128)(2,1)} %bitcast.7, bf16[12,128,512]{2,1,0:T(8,128)(2,1)} %bitcast.13, bf16[12,128,512]{2,1,0:T(8,128)(2,1)} %copy-done.3), custom_call_target="tpu_custom_call" | custom-call | flops 2000000000 | bytes 5000000 | tf_op jit(solution)/shard_map/reads/pallas_call | solution.py:379
  50.8 0.0 collective-permute-done.4.refs_7_
  50.8 0.0 copy-start.6
  50.8 0.0 collective-permute-done.3.refs_5_
  50.8 0.0 copy-start.4
  50.8 0.6 copy-done.6
  51.4 0.2 copy-done.4
  51.6 10.7 %finish.1 = bf16[1024,256]{1,0:T(8,128)(2,1)} custom-call(f32[1,256]{1,0:T(1,128)} %bitcast.14, f32[512,256]{1,0:T(8,128)} %get-tuple-element.22.refs_1_, f32[512,256]{1,0:T(8,128)} %get-tuple-element.28.refs_2_, f32[512,256]{1,0:T(8,128)} %get-tuple-element.29.refs_3_, f32[512,256]{1,0:T(8,128)} %get-tuple-element.30.refs_4_, ...), custom_call_target="tpu_custom_call" | custom-call | flops 1000000000 | bytes 6000000 | tf_op jit(solution)/shard_map/finish/pallas_call | solution.py:414
  62.4 1.9 %copy.20 = bf16[1024,256]{1,0:T(8,128)(2,1)} copy(bf16[1024,256]{1,0:T(8,128)(2,1)} %finish.1) | data formatting | bytes 1048576
Async XLA Ops:
  4.2 8.1 %copy-start = (bf16[1024,256]{1,0:T(8,128)(2,1)S(1)}, bf16[1024,256]{1,0:T(8,128)(2,1)}, u32[]{:S(2)}) copy-start(bf16[1024,256]{1,0:T(8,128)(2,1)} %query.1) | copy-start | bytes 1572868
  4.2 10.6 %copy-start.2 = (s32[8,4]{0,1:T(4,128)S(1)}, s32[8,4]{0,1:T(4,128)}, u32[]{:S(2)}) copy-start(s32[8,4]{0,1:T(4,128)} %param.31) | copy-start | bytes 388
  11.7 15.7 %collective-permute-start.2 = (bf16[12,128,512]{2,1,0:T(8,128)(2,1)}, bf16[12,128,512]{2,1,0:T(8,128)(2,1)S(1)}, u32[]{:S(2)}, u32[]{:S(2)}) collective-permute-start(bf16[12,128,512]{2,1,0:T(8,128)(2,1)} %bitcast.11), channel_id=1, source_target_pairs={{0,4},{4,0},{8,12},{12,8},{1,5},{5,1},{9,13},{13,9},{2,6},{6,2},{1... | collective-permute-start | bytes 4718600 | tf_op jit(solution)/shard_map/ppermute | solution.py:336
  12.2 15.2 %collective-permute-start.1 = (bf16[8,128,256]{2,1,0:T(8,128)(2,1)S(1)}, bf16[8,128,256]{2,1,0:T(8,128)(2,1)S(1)}, u32[]{:S(2)}, u32[]{:S(2)}) collective-permute-start(bf16[8,128,256]{2,1,0:T(8,128)(2,1)S(1)} %bitcast.8), channel_id=1, source_target_pairs={{0,8},{4,12},{8,0},{12,4},{1,9},{5,13},{9,1},{13,5},{2,10},{6,14},... | collective-permute-start | bytes 1572872 | tf_op jit(solution)/shard_map/ppermute | solution.py:299
  14.9 8.6 %copy-start.1 = (s32[8,4]{1,0:T(8,128)}, s32[8,4]{1,0:T(8,128)S(1)}, u32[]{:S(2)}) copy-start(s32[8,4]{1,0:T(8,128)S(1)} %copy.17.ids_ref) | copy-start | bytes 388
  14.9 12.5 %collective-permute-start = (s32[8,4]{1,0:T(8,128)S(1)}, s32[8,4]{1,0:T(8,128)S(1)}, u32[]{:S(2)}, u32[]{:S(2)}) collective-permute-start(s32[8,4]{1,0:T(8,128)S(1)} %copy.17.ids_ref), channel_id=1, source_target_pairs={{0,8},{4,12},{8,0},{12,4},{1,9},{5,13},{9,1},{13,5},{2,10},{6,14},... | collective-permute-start | bytes 392 | tf_op jit(solution)/shard_map/ppermute | solution.py:299
  27.4 0.6 copy-start.7
  27.4 0.8 %copy-start.5 = (bf16[8,128,256]{2,1,0:T(8,128)(2,1)}, bf16[8,128,256]{2,1,0:T(8,128)(2,1)S(1)}, u32[]{:S(2)}) copy-start(bf16[8,128,256]{2,1,0:T(8,128)(2,1)S(1)} %collective-permute-done.1.q_ref) | copy-start | bytes 1572868
  28.2 1.1 %copy-start.3 = (bf16[12,128,512]{2,1,0:T(8,128)(2,1)}, bf16[12,128,512]{2,1,0:T(8,128)(2,1)S(1)}, u32[]{:S(2)}) copy-start(bf16[12,128,512]{2,1,0:T(8,128)(2,1)S(1)} %collective-permute-done.2.other_ref) | copy-start | bytes 4718596
  35.1 15.7 %collective-permute-start.3 = (bf16[8,128,256]{2,1,0:T(8,128)(2,1)}, bf16[8,128,256]{2,1,0:T(8,128)(2,1)S(1)}, u32[]{:S(2)}, u32[]{:S(2)}) collective-permute-start(bf16[8,128,256]{2,1,0:T(8,128)(2,1)} %get-tuple-element.24), channel_id=1, source_target_pairs={{0,8},{4,12},{8,0},{12,4},{1,9},{5,13},{9,1},{13,5},{2,10},{6,14},... | collective-permute-start | bytes 1572872 | tf_op jit(solution)/shard_map/ppermute | solution.py:299
  36.9 13.9 %collective-permute-start.4 = (f32[2,8,128]{2,1,0:T(8,128)}, f32[2,8,128]{2,1,0:T(8,128)S(1)}, u32[]{:S(2)}, u32[]{:S(2)}) collective-permute-start(f32[2,8,128]{2,1,0:T(8,128)} %get-tuple-element.33), channel_id=1, source_target_pairs={{0,8},{4,12},{8,0},{12,4},{1,9},{5,13},{9,1},{13,5},{2,10},{6,14},... | collective-permute-start | bytes 24584 | tf_op jit(solution)/shard_map/ppermute | solution.py:299
  50.8 0.6 copy-start.6
  50.8 0.8 %copy-start.4 = (bf16[8,128,256]{2,1,0:T(8,128)(2,1)}, bf16[8,128,256]{2,1,0:T(8,128)(2,1)S(1)}, u32[]{:S(2)}) copy-start(bf16[8,128,256]{2,1,0:T(8,128)(2,1)S(1)} %collective-permute-done.3.refs_5_) | copy-start | bytes 1572868
